TPU v7x, 32 devices: a whole 2x2x4 slice. The times are simulated.
32 devices in a mesh: grp: 2 (over y), fs: 4 (over z), tp: 4 (over x, core).
Axes of the slice: x: 2, y: 2, z: 4, core: 2. Of those that a mesh axis runs over, the one named last changes fastest.
Arguments:
- tokens: bfloat16 [2048, 2048], P(('grp', 'fs', 'tp')), parts along dimension 0, may hold values from -30 to 30
- gate_master: float32 [2048, 2752], P('fs', 'tp'), may hold values from -0.125 to 0.125
- up_master: float32 [2048, 2752], P('fs', 'tp'), may hold values from -0.125 to 0.125
- down_master: float32 [2048, 2752], P('fs', 'tp'), may hold values from -0.4375 to 0.4375
- norm_gain: float32 [2048], replicated, may hold values from 0.1 to 1.9
- post_gain: float32 [2048], replicated, may hold values from 0.1 to 1.9
- post_bias: float32 [2048], replicated, may hold values from -3 to 3
Outputs:
- gate_ready: bfloat16 [4096, 2752], P('grp', 'tp'), parts along dimension 0
- up_ready: bfloat16 [4096, 2752], P('grp', 'tp'), parts along dimension 0
- down_ready: bfloat16 [4096, 2752], P('grp', 'tp'), parts along dimension 0
- result: bfloat16 [2048, 2048], P(('grp', 'fs', 'tp')), parts along dimension 0
There are 2 independent parts, one for each index of `grp`. A program takes and returns all parts, laid end to end along the dimension named above; an argument that names none is the same for every part. Nothing has to cross between parts.
All inputs are finite; a program needn't handle non-finite values.
Results may differ from a plain program's by a relative error of at most 0.009.
Values may be sent and summed in bfloat16 or wider, within the bound.
A program may use at most 64 MiB of HBM per device.

v0:
```python
import functools

import jax
import jax.numpy as jnp
from jax import lax
from jax.experimental import pallas as pl
from jax.experimental.pallas import tpu as pltpu
from jax.sharding import PartitionSpec as P

MESH = pl.DeviceIdType.MESH
LANES = 128


def finish(wide, branch, post_gain, post_bias):
    mixed = jnp.sqrt(jnp.float32(2.0)) * wide + 0.5 * branch
    center = jnp.mean(mixed, axis=-1, keepdims=True)
    spread = jnp.mean(jnp.square(mixed - center), axis=-1, keepdims=True)
    return ((mixed - center) * lax.rsqrt(spread + 1e-05) * post_gain + post_bias).astype(
        jnp.bfloat16
    )


def plain(tokens, gate_master, up_master, down_master, norm_gain, post_gain, post_bias):
    row_count = gate_master.shape[0]
    first_row = lax.axis_index("fs") * row_count
    gain_rows = lax.dynamic_slice_in_dim(norm_gain, first_row, row_count, 0)
    gate_piece = (gain_rows[:, None] * gate_master).astype(jnp.bfloat16)
    up_piece = (gain_rows[:, None] * up_master).astype(jnp.bfloat16)
    down_piece = down_master.astype(jnp.bfloat16)
    gate_ready, up_ready, down_ready = (
        lax.all_gather(gate_piece, "fs", axis=0, tiled=True),
        lax.all_gather(up_piece, "fs", axis=0, tiled=True),
        lax.all_gather(down_piece, "fs", axis=0, tiled=True),
    )
    wide = tokens.astype(jnp.float32)
    normed = (wide * lax.rsqrt(jnp.mean(wide * wide, axis=-1, keepdims=True) + 1e-06)).astype(
        jnp.bfloat16
    )
    piece = lax.all_gather(normed, "tp", axis=0, tiled=True)
    gate = jnp.dot(piece, gate_ready, preferred_element_type=jnp.float32)
    upward = jnp.dot(piece, up_ready, preferred_element_type=jnp.float32)
    hidden = (jax.nn.silu(gate) * upward).astype(jnp.bfloat16)
    branch = lax.psum_scatter(
        lax.dot_general(
            hidden, down_ready, (((1,), (1,)), ((), ())), preferred_element_type=jnp.float32
        ).astype(jnp.bfloat16),
        "tp",
        scatter_dimension=0,
        tiled=True,
    ).astype(jnp.float32)
    result = finish(wide, branch, post_gain, post_bias)
    return (gate_ready, up_ready, down_ready, result)


def fused_kernel(
    fs, tp, n, tok_ref, gm_ref, um_ref, dm_ref, gain_ref, pg_ref, pb_ref,
    go_ref, uo_ref, do_ref, res_ref,
    stage, fg, fu, fd, toks, acc_g, acc_u, hid, parts, got, mixed,
    up_sem, dn_sem, y_sem, r_sem, ts_sem, tr_sem, ps_sem, pr_sem, o_sem, i_sem,
):
    y, z, t = lax.axis_index("grp"), lax.axis_index("fs"), lax.axis_index("tp")
    cols, rc = gm_ref.shape
    tok_rows, d = tok_ref.shape
    tiles = d // LANES
    full = (fg, fu, fd)
    outs = (go_ref, uo_ref, do_ref)
    masters = (gm_ref, um_ref, dm_ref)
    up_dev = (y, jnp.minimum(z + 1, fs - 1), t)
    dn_dev = (y, jnp.maximum(z - 1, 0), t)
    y_dev = (1 - y, z, t)
    has_up, has_dn = z < fs - 1, z > 0
    peers = [lax.rem(t + j, tp) for j in range(1, tp)]
    first = [(m, c) for m in (0, 1) for c in range(n)]
    second = [(2, c) for c in range(n)]

    def fetch(m, h, c):
        k = h * n + c
        return pltpu.make_async_copy(
            masters[m].at[:, pl.ds(pl.multiple_of(k * LANES, LANES), LANES)],
            stage.at[m, k], i_sem.at[m, k],
        )

    for h in (y, 1 - y):
        for m, c in first + second:
            fetch(m, h, c).start()

    barrier = pltpu.get_barrier_semaphore()

    def greet(dev):
        pl.semaphore_signal(barrier, inc=1, device_id=dev, device_id_type=MESH)

    pl.when(has_up)(lambda: greet(up_dev))
    pl.when(has_dn)(lambda: greet(dn_dev))
    greet(y_dev)
    for peer in peers:
        greet((y, z, peer))

    def tile_of(b, h, c):
        return b * (2 * n) + h * n + c

    def hop(m, k, dev, sem):
        s = m * tiles + k
        return pltpu.make_async_remote_copy(
            src_ref=full[m].at[k], dst_ref=full[m].at[k], send_sem=sem.at[s], recv_sem=r_sem.at[s],
            device_id=dev, device_id_type=MESH,
        )

    def put_out(m, k):
        pltpu.make_async_copy(
            full[m].at[k],
            outs[m].at[:, pl.ds(pl.multiple_of(k * LANES, LANES), LANES)],
            o_sem.at[m, k],
        ).start()

    def keep(m, h, c):
        fetch(m, h, c).wait()
        k = tile_of(z, h, c)
        v = stage[m, h * n + c]
        if m < 2:
            v = v * gain_ref[:, pl.ds(pl.multiple_of(k * LANES, LANES), LANES)]
        full[m][k] = v.astype(jnp.bfloat16)

    def send_own(m, c):
        k = tile_of(z, y, c)
        pl.when(has_up)(lambda: hop(m, k, up_dev, up_sem).start())
        pl.when(has_dn)(lambda: hop(m, k, dn_dev, dn_sem).start())

    def part_copy(k, j, peer):
        return pltpu.make_async_remote_copy(
            src_ref=parts.at[k, pl.ds(pl.multiple_of(peer * tok_rows, tok_rows), tok_rows)],
            dst_ref=got.at[t, k],
            send_sem=ps_sem.at[j, k], recv_sem=pr_sem.at[t, k],
            device_id=(y, z, peer), device_id_type=MESH,
        )

    def down_tile(k):
        part = jnp.dot(hid[...], fd[k], preferred_element_type=jnp.float32)
        parts[k] = part.astype(jnp.bfloat16)
        for j, peer in enumerate(peers):
            part_copy(k, j, peer).start()

    def add_tiles(m, k, start):
        acc = (acc_g, acc_u)[m]
        at = pl.ds(pl.multiple_of(k * LANES, LANES), n * LANES)
        lhs = toks[:, :, at].reshape(tp * tok_rows, n * LANES)
        rhs = jnp.concatenate([full[m][k + i] for i in range(n)], axis=1)
        term = lax.dot_general(
            lhs, rhs, (((1,), (1,)), ((), ())), preferred_element_type=jnp.float32
        )
        acc[...] = term if start else acc[...] + term

    def ends(p):
        low, high = z - 1 - p, z + 1 + p
        return ((low, low >= 0), (high, high <= fs - 1))

    sums, downs = [], []

    def later(m, b, ok, h, c):
        if m == 2:
            downs.append((ok, lambda: down_tile(tile_of(b, h, c))))
        elif c == n - 1:
            sums.append((ok, lambda: add_tiles(m, tile_of(b, h, 0), False)))

    def work(todo, count):
        for _ in range(min(count, len(todo))):
            ok, item = todo.pop(0)
            if ok is None:
                item()
            else:
                pl.when(ok)(item)

    def arrived(m, c, p):
        (low, has_low), (high, has_high) = ends(p)

        @pl.when(has_low)
        def _():
            k = tile_of(low, y, c)
            hop(m, k, up_dev, up_sem).wait_recv()
            hop(m, k, y_dev, y_sem).start()
            pl.when(has_up)(lambda: hop(m, k, up_dev, up_sem).start())
            put_out(m, k)

        @pl.when(has_high)
        def _():
            k = tile_of(high, y, c)
            hop(m, k, dn_dev, dn_sem).wait_recv()
            hop(m, k, y_dev, y_sem).start()
            pl.when(has_dn)(lambda: hop(m, k, dn_dev, dn_sem).start())
            put_out(m, k)

        for b, ok in ends(p):
            later(m, b, ok, y, c)

    def crossed(m, c, p):
        for b, ok in ends(p):
            @pl.when(ok)
            def _(b=b):
                k = tile_of(b, 1 - y, c)
                hop(m, k, y_dev, y_sem).wait_recv()
                put_out(m, k)
            later(m, b, ok, 1 - y, c)

    def tok_copy(j, peer, origin):
        return pltpu.make_async_remote_copy(
            src_ref=toks.at[origin], dst_ref=toks.at[origin],
            send_sem=ts_sem.at[j], recv_sem=tr_sem.at[origin],
            device_id=(y, z, peer), device_id_type=MESH,
        )

    wide = tok_ref[...].astype(jnp.float32)
    scale = lax.rsqrt(jnp.mean(wide * wide, axis=-1, keepdims=True) + 1e-06)
    toks[t] = (wide * scale).astype(jnp.bfloat16)
    keep(first[0][0], y, first[0][1])
    expected = has_up.astype(jnp.int32) + has_dn.astype(jnp.int32) + tp
    pl.semaphore_wait(barrier, expected)
    for before, pair in zip(first, first[1:]):
        keep(pair[0], y, pair[1])
        send_own(*before)
    for m, c in second:
        keep(m, y, c)
    send_own(*first[-1])
    for j, peer in enumerate(peers):
        tok_copy(j, peer, t).start()
    for m, c in first + second:
        keep(m, 1 - y, c)
    for m, c in first + second:
        for h in range(2):
            put_out(m, tile_of(z, h, c))

    waiting = []
    for p in range(fs - 1):
        for m, c in first:
            arrived(m, c, p)
            waiting.append((m, c, p))
            if len(waiting) > 2 * len(first):
                crossed(*waiting.pop(0))
            if p > 0:
                work(sums, 4)
        if p == 0:
            for j, peer in enumerate(peers):
                tok_copy(j, peer, peer).wait_recv()
            own = [
                (None, lambda m=m, h=h: add_tiles(m, tile_of(z, h, 0), h == 0))
                for m in (0, 1) for h in (0, 1)
            ]
            sums[:0] = own
    for pair in second:
        send_own(*pair)
    for p in range(fs - 1):
        for m, c in second:
            arrived(m, c, p)
            waiting.append((m, c, p))
            if p > 0 and len(waiting) > 2:
                crossed(*waiting.pop(0))
            work(downs if p > 0 else sums, 4)
        if p == 0:
            while waiting[0][0] < 2:
                crossed(*waiting.pop(0))
            work(sums, len(sums))
            hid[...] = (jax.nn.silu(acc_g[...]) * acc_u[...]).astype(jnp.bfloat16)
            downs[:0] = [
                (None, lambda h=h, c=c: down_tile(tile_of(z, h, c)))
                for h in (0, 1) for c in range(n)
            ]
    while waiting:
        crossed(*waiting.pop(0))
    work(downs, len(downs))

    wide = tok_ref[...].astype(jnp.float32)
    mine = pl.ds(pl.multiple_of(t * tok_rows, tok_rows), tok_rows)
    for k in range(tiles):
        branch = parts[k, mine, :].astype(jnp.float32)
        for j, peer in enumerate(peers):
            pltpu.make_async_remote_copy(
                src_ref=got.at[peer, k], dst_ref=got.at[peer, k],
                send_sem=ps_sem.at[j, k], recv_sem=pr_sem.at[peer, k],
                device_id=(y, z, peer), device_id_type=MESH,
            ).wait_recv()
            branch = branch + got[peer, k].astype(jnp.float32)
        at = slice(k * LANES, (k + 1) * LANES)
        mixed[:, at] = jnp.sqrt(jnp.float32(2.0)) * wide[:, at] + 0.5 * branch
    mix = mixed[...]
    center = jnp.mean(mix, axis=-1, keepdims=True)
    off = mix - center
    spread = jnp.mean(jnp.square(off), axis=-1, keepdims=True)
    res_ref[...] = (
        off * lax.rsqrt(spread + 1e-05) * pg_ref[...] + pb_ref[...]
    ).astype(jnp.bfloat16)

    for j, peer in enumerate(peers):
        tok_copy(j, peer, t).wait_send()
        for k in range(tiles):
            part_copy(k, j, peer).wait_send()
    for m in range(3):
        for k in range(tiles):
            pltpu.make_async_copy(
                full[m].at[k], outs[m].at[:, k * LANES:(k + 1) * LANES], o_sem.at[m, k]
            ).wait()
        for c in range(n):
            for b in range(fs):
                k = tile_of(b, y, c)
                pl.when(has_up & (b <= z))(lambda k=k: hop(m, k, up_dev, up_sem).wait_send())
                pl.when(has_dn & (b >= z))(lambda k=k: hop(m, k, dn_dev, dn_sem).wait_send())
                pl.when(z != b)(lambda k=k: hop(m, k, y_dev, y_sem).wait_send())


def fused(fs, tp, n, tokens, gate_master, up_master, down_master, norm_gain, post_gain, post_bias):
    rc, cols = gate_master.shape
    tok_rows, d = tokens.shape
    tiles, rows = d // LANES, tp * tok_rows
    bf, f32 = jnp.bfloat16, jnp.float32
    ready = jax.ShapeDtypeStruct((cols, d), bf)
    vmem = pl.BlockSpec(memory_space=pltpu.VMEM)
    anywhere = pl.BlockSpec(memory_space=pl.ANY)
    dma = pltpu.SemaphoreType.DMA
    gate, up, down, result = pl.pallas_call(
        functools.partial(fused_kernel, fs, tp, n),
        out_shape=(ready, ready, ready, jax.ShapeDtypeStruct((tok_rows, d), bf)),
        in_specs=[vmem] + [anywhere] * 3 + [vmem] * 3,
        out_specs=(anywhere, anywhere, anywhere, vmem),
        scratch_shapes=[
            pltpu.VMEM((3, 2 * n, cols, LANES), f32),
            pltpu.VMEM((tiles, cols, LANES), bf),
            pltpu.VMEM((tiles, cols, LANES), bf),
            pltpu.VMEM((tiles, cols, LANES), bf),
            pltpu.VMEM((tp, tok_rows, d), bf),
            pltpu.VMEM((rows, cols), f32),
            pltpu.VMEM((rows, cols), f32),
            pltpu.VMEM((rows, cols), bf),
            pltpu.VMEM((tiles, rows, LANES), bf),
            pltpu.VMEM((tp, tiles, tok_rows, LANES), bf),
            pltpu.VMEM((tok_rows, d), f32),
            dma((3 * tiles,)), dma((3 * tiles,)), dma((3 * tiles,)), dma((3 * tiles,)),
            dma((tp - 1,)), dma((tp,)),
            dma((tp - 1, tiles)), dma((tp, tiles)), dma((3, tiles)), dma((3, 2 * n)),
        ],
        compiler_params=pltpu.CompilerParams(
            collective_id=0, has_side_effects=True, vmem_limit_bytes=60 * 2**20
        ),
    )(
        tokens, gate_master.T, up_master.T, down_master.T, norm_gain[None, :],
        post_gain[None, :], post_bias[None, :],
    )
    return gate.T, up.T, down.T, result


def solution(mesh):
    grp, fs, tp = mesh.shape["grp"], mesh.shape["fs"], mesh.shape["tp"]

    def local(tokens, gate_master, *rest):
        rc, cols = gate_master.shape
        n = rc // (2 * LANES)
        fits = grp == 2 and fs > 1 and rc % (2 * LANES) == 0 and 2 * n * fs <= 32
        fits = fits and cols % 16 == 0 and tokens.shape[0] % 16 == 0
        if fits:
            return fused(fs, tp, n, tokens, gate_master, *rest)
        return plain(tokens, gate_master, *rest)

    return jax.shard_map(
        local,
        mesh=mesh,
        in_specs=(
            P(("grp", "fs", "tp"), None),
            P("fs", "tp"),
            P("fs", "tp"),
            P("fs", "tp"),
            P(),
            P(),
            P(),
        ),
        out_specs=(P("grp", "tp"), P("grp", "tp"), P("grp", "tp"), P(("grp", "fs", "tp"), None)),
        check_vma=False,
    )
```

profile of v0, /device:TPU:0, one launch (start us, length us, event | category | flops | bytes accessed | tf_op | source)
XLA Modules:
  0.0 99.4 jit_solution(16190318883525150280)
XLA Ops:
  0.6 89.8 %shard_map.102 = (bf16[688,2048]{1,0:T(8,128)(2,1)}, bf16[688,2048]{1,0:T(8,128)(2,1)}, bf16[688,2048]{1,0:T(8,128)(2,1)}, bf16[64,2048]{1,0:T(8,128)(2,1)}) custom-call(bf16[64,2048]{1,0:T(8,128)(2,1)} %tok_ref.1, f32[688,512]{1,0:T(8,128)} %bitcast.12, f32[688,512]{1,0:T(8,128)} %bitcast.13, f32[688,512]{1,0:T(8,128)} %bitcast.14, f32[1,2048]{1,0:T(1,128)} %bitcast.15, ...), custom_call_target="tpu_custom_call" | custom-call | tf_op jit(solution)/shard_map/pallas_call | solution.py:316
  90.5 0.0 copy-start.1
  90.5 3.9 %copy.15 = bf16[2048,688]{0,1:T(8,128)(2,1)} copy(bf16[2048,688]{0,1:T(8,128)(2,1)} %bitcast.11) | data formatting | bytes 5636096
  94.3 0.0 copy-done.1
  94.3 0.0 copy-start
  94.3 1.6 %copy.16 = bf16[2048,688]{0,1:T(8,128)(2,1)} copy(bf16[2048,688]{0,1:T(8,128)(2,1)S(1)} %bitcast.10) | data formatting | bytes 5636096
  95.9 1.3 %copy-done = bf16[688,2048]{1,0:T(8,128)(2,1)S(1)} copy-done((bf16[688,2048]{1,0:T(8,128)(2,1)S(1)}, bf16[688,2048]{1,0:T(8,128)(2,1)}, u32[]{:S(2)}) %copy-start) | copy-done | bytes 2818072
  97.2 0.0 copy-start.2
  97.2 1.6 %copy.17 = bf16[2048,688]{0,1:T(8,128)(2,1)} copy(bf16[2048,688]{0,1:T(8,128)(2,1)S(1)} %bitcast.9) | data formatting | bytes 5636096
  98.7 0.0 copy-done.2
  98.7 0.7 copy.18
Async XLA Ops:
  90.5 3.9 %copy-start.1 = (bf16[688,2048]{1,0:T(8,128)(2,1)S(1)}, bf16[688,2048]{1,0:T(8,128)(2,1)}, u32[]{:S(2)}) copy-start(bf16[688,2048]{1,0:T(8,128)(2,1)} %get-tuple-element.9) | copy-start | bytes 8454148
  94.3 2.8 %copy-start = (bf16[688,2048]{1,0:T(8,128)(2,1)S(1)}, bf16[688,2048]{1,0:T(8,128)(2,1)}, u32[]{:S(2)}) copy-start(bf16[688,2048]{1,0:T(8,128)(2,1)} %get-tuple-element.10) | copy-start | bytes 8454148
  97.2 1.6 %copy-start.2 = (bf16[64,2048]{1,0:T(8,128)(2,1)S(1)}, bf16[64,2048]{1,0:T(8,128)(2,1)}, u32[]{:S(2)}) copy-start(bf16[64,2048]{1,0:T(8,128)(2,1)} %get-tuple-element.19) | copy-start | bytes 786436
where the time goes:
time: 99.6 us; the launch traced here: 99.4 us
  Pallas kernels  89.8 us (90%)
  local copies, waits for them, and re-layouts  8.94 us (9%)
    pallas_call x1, Pallas kernels, fused(): pl.pallas_call(functools.partial(fused_kernel, fs, tp, n), out_shape=(rea...  89.8 us
    unnamed x10, local copies, waits for them, and re-layouts  8.94 us

commit v1 on v0

--- a/solution.py
+++ b/solution.py
@@ -53,17 +53,16 @@
 
 
 def fused_kernel(
-    fs, tp, n, tok_ref, gm_ref, um_ref, dm_ref, gain_ref, pg_ref, pb_ref,
-    go_ref, uo_ref, do_ref, res_ref,
-    stage, fg, fu, fd, toks, acc_g, acc_u, hid, parts, got, mixed,
-    up_sem, dn_sem, y_sem, r_sem, ts_sem, tr_sem, ps_sem, pr_sem, o_sem, i_sem,
+    fs, tp, n, tok_ref, gm_ref, um_ref, dm_ref, gain_ref,
+    fg, fu, fd, mixed,
+    stage, toks, acc_g, acc_u, hid, parts, got,
+    up_sem, dn_sem, y_sem, r_sem, ts_sem, tr_sem, ps_sem, pr_sem, i_sem,
 ):
     y, z, t = lax.axis_index("grp"), lax.axis_index("fs"), lax.axis_index("tp")
     cols, rc = gm_ref.shape
     tok_rows, d = tok_ref.shape
     tiles = d // LANES
     full = (fg, fu, fd)
-    outs = (go_ref, uo_ref, do_ref)
     masters = (gm_ref, um_ref, dm_ref)
     up_dev = (y, jnp.minimum(z + 1, fs - 1), t)
     dn_dev = (y, jnp.maximum(z - 1, 0), t)
@@ -105,13 +104,6 @@
             device_id=dev, device_id_type=MESH,
         )
 
-    def put_out(m, k):
-        pltpu.make_async_copy(
-            full[m].at[k],
-            outs[m].at[:, pl.ds(pl.multiple_of(k * LANES, LANES), LANES)],
-            o_sem.at[m, k],
-        ).start()
-
     def keep(m, h, c):
         fetch(m, h, c).wait()
         k = tile_of(z, h, c)
@@ -178,7 +170,6 @@
             hop(m, k, up_dev, up_sem).wait_recv()
             hop(m, k, y_dev, y_sem).start()
             pl.when(has_up)(lambda: hop(m, k, up_dev, up_sem).start())
-            put_out(m, k)
 
         @pl.when(has_high)
         def _():
@@ -186,7 +177,6 @@
             hop(m, k, dn_dev, dn_sem).wait_recv()
             hop(m, k, y_dev, y_sem).start()
             pl.when(has_dn)(lambda: hop(m, k, dn_dev, dn_sem).start())
-            put_out(m, k)
 
         for b, ok in ends(p):
             later(m, b, ok, y, c)
@@ -197,7 +187,6 @@
             def _(b=b):
                 k = tile_of(b, 1 - y, c)
                 hop(m, k, y_dev, y_sem).wait_recv()
-                put_out(m, k)
             later(m, b, ok, 1 - y, c)
 
     def tok_copy(j, peer, origin):
@@ -223,10 +212,6 @@
         tok_copy(j, peer, t).start()
     for m, c in first + second:
         keep(m, 1 - y, c)
-    for m, c in first + second:
-        for h in range(2):
-            put_out(m, tile_of(z, h, c))
-
     waiting = []
     for p in range(fs - 1):
         for m, c in first:
@@ -279,29 +264,38 @@
             branch = branch + got[peer, k].astype(jnp.float32)
         at = slice(k * LANES, (k + 1) * LANES)
         mixed[:, at] = jnp.sqrt(jnp.float32(2.0)) * wide[:, at] + 0.5 * branch
-    mix = mixed[...]
+
+    for j, peer in enumerate(peers):
+        tok_copy(j, peer, t).wait_send()
+        for k in range(tiles):
+            part_copy(k, j, peer).wait_send()
+    for m in range(3):
+        for c in range(n):
+            for b in range(fs):
+                k = tile_of(b, y, c)
+                pl.when(has_up & (b <= z))(lambda k=k: hop(m, k, up_dev, up_sem).wait_send())
+                pl.when(has_dn & (b >= z))(lambda k=k: hop(m, k, dn_dev, dn_sem).wait_send())
+                pl.when(z != b)(lambda k=k: hop(m, k, y_dev, y_sem).wait_send())
+
+
+def emit_kernel(fg, fu, fd, mixed_ref, pg_ref, pb_ref, go_ref, uo_ref, do_ref, res_ref, sem):
+    tiles = fg.shape[0]
+    copies = [
+        pltpu.make_async_copy(src.at[k], out.at[:, k * LANES:(k + 1) * LANES], sem.at[m, k])
+        for m, (src, out) in enumerate(((fg, go_ref), (fu, uo_ref), (fd, do_ref)))
+        for k in range(tiles)
+    ]
+    for copy in copies:
+        copy.start()
+    mix = mixed_ref[...]
     center = jnp.mean(mix, axis=-1, keepdims=True)
     off = mix - center
     spread = jnp.mean(jnp.square(off), axis=-1, keepdims=True)
     res_ref[...] = (
         off * lax.rsqrt(spread + 1e-05) * pg_ref[...] + pb_ref[...]
     ).astype(jnp.bfloat16)
-
-    for j, peer in enumerate(peers):
-        tok_copy(j, peer, t).wait_send()
-        for k in range(tiles):
-            part_copy(k, j, peer).wait_send()
-    for m in range(3):
-        for k in range(tiles):
-            pltpu.make_async_copy(
-                full[m].at[k], outs[m].at[:, k * LANES:(k + 1) * LANES], o_sem.at[m, k]
-            ).wait()
-        for c in range(n):
-            for b in range(fs):
-                k = tile_of(b, y, c)
-                pl.when(has_up & (b <= z))(lambda k=k: hop(m, k, up_dev, up_sem).wait_send())
-                pl.when(has_dn & (b >= z))(lambda k=k: hop(m, k, dn_dev, dn_sem).wait_send())
-                pl.when(z != b)(lambda k=k: hop(m, k, y_dev, y_sem).wait_send())
+    for copy in copies:
+        copy.wait()
 
 
 def fused(fs, tp, n, tokens, gate_master, up_master, down_master, norm_gain, post_gain, post_bias):
@@ -309,38 +303,48 @@
     tok_rows, d = tokens.shape
     tiles, rows = d // LANES, tp * tok_rows
     bf, f32 = jnp.bfloat16, jnp.float32
-    ready = jax.ShapeDtypeStruct((cols, d), bf)
+    held = pltpu.VMEM((tiles, cols, LANES), bf)
     vmem = pl.BlockSpec(memory_space=pltpu.VMEM)
     anywhere = pl.BlockSpec(memory_space=pl.ANY)
     dma = pltpu.SemaphoreType.DMA
-    gate, up, down, result = pl.pallas_call(
+    kept = pl.pallas_call(
         functools.partial(fused_kernel, fs, tp, n),
-        out_shape=(ready, ready, ready, jax.ShapeDtypeStruct((tok_rows, d), bf)),
-        in_specs=[vmem] + [anywhere] * 3 + [vmem] * 3,
-        out_specs=(anywhere, anywhere, anywhere, vmem),
+        out_shape=(held, held, held, pltpu.VMEM((tok_rows, d), f32)),
+        in_specs=[vmem] + [anywhere] * 3 + [vmem],
+        out_specs=(vmem,) * 4,
         scratch_shapes=[
             pltpu.VMEM((3, 2 * n, cols, LANES), f32),
-            pltpu.VMEM((tiles, cols, LANES), bf),
-            pltpu.VMEM((tiles, cols, LANES), bf),
-            pltpu.VMEM((tiles, cols, LANES), bf),
             pltpu.VMEM((tp, tok_rows, d), bf),
             pltpu.VMEM((rows, cols), f32),
             pltpu.VMEM((rows, cols), f32),
             pltpu.VMEM((rows, cols), bf),
             pltpu.VMEM((tiles, rows, LANES), bf),
             pltpu.VMEM((tp, tiles, tok_rows, LANES), bf),
-            pltpu.VMEM((tok_rows, d), f32),
             dma((3 * tiles,)), dma((3 * tiles,)), dma((3 * tiles,)), dma((3 * tiles,)),
             dma((tp - 1,)), dma((tp,)),
-            dma((tp - 1, tiles)), dma((tp, tiles)), dma((3, tiles)), dma((3, 2 * n)),
+            dma((tp - 1, tiles)), dma((tp, tiles)), dma((3, 2 * n)),
         ],
         compiler_params=pltpu.CompilerParams(
-            collective_id=0, has_side_effects=True, vmem_limit_bytes=60 * 2**20
+            collective_id=0, has_side_effects=True, vmem_limit_bytes=50 * 2**20
         ),
     )(
-        tokens, gate_master.T, up_master.T, down_master.T, norm_gain[None, :],
-        post_gain[None, :], post_bias[None, :],
-    )
+        tokens,
+        *(
+            pltpu.with_memory_space_constraint(x.T, pltpu.HBM)
+            for x in (gate_master, up_master, down_master)
+        ),
+        norm_gain[None, :],
+    )
+    kept = [pltpu.with_memory_space_constraint(x, pltpu.VMEM) for x in kept]
+    ready = jax.ShapeDtypeStruct((cols, d), bf)
+    gate, up, down, result = pl.pallas_call(
+        emit_kernel,
+        out_shape=(ready, ready, ready, jax.ShapeDtypeStruct((tok_rows, d), bf)),
+        in_specs=[vmem] * 6,
+        out_specs=(anywhere, anywhere, anywhere, vmem),
+        scratch_shapes=[dma((3, tiles))],
+        compiler_params=pltpu.CompilerParams(vmem_limit_bytes=20 * 2**20),
+    )(*kept, post_gain[None, :], post_bias[None, :])
     return gate.T, up.T, down.T, result
 
 

time: 99.6 us -> 93.6 us (0.940)
  local copies, waits for them, and re-layouts: 8.94 us -> 0.01 us
  Pallas kernels: 89.8 us -> 92.8 us
    unnamed x10 -> x4, local copies, waits for them, and re-layouts: 8.94 us -> 0.01 us
    pallas_call x1 -> x2, Pallas kernels: 89.8 us -> 92.8 us  [the longest x1 88.3 us: fused(): pl.pallas_call(functools.partial(fused_kernel, fs, tp, n), out_shape=(hel...]
where the time goes in v1:
time: 93.6 us; the launch traced here: 93.4 us
  Pallas kernels  92.8 us (99%)
    pallas_call x1, Pallas kernels, fused(): pl.pallas_call(functools.partial(fused_kernel, fs, tp, n), out_shape=(hel...  88.3 us
    pallas_call x1, Pallas kernels, fused(): pl.pallas_call(emit_kernel, out_shape=(ready, ready, ready, jax.ShapeDtyp...  4.43 us

profile of v1, /device:TPU:0, one launch (start us, length us, event | category | flops | bytes accessed | tf_op | source)
XLA Modules:
  0.0 93.4 jit_solution(14716445829215878518)
XLA Ops:
  0.6 0.0 copy-start.1
  0.6 0.0 copy-start
  0.7 88.3 %shard_map.102 = (bf16[16,688,128]{2,1,0:T(8,128)(2,1)S(1)}, bf16[16,688,128]{2,1,0:T(8,128)(2,1)S(1)}, bf16[16,688,128]{2,1,0:T(8,128)(2,1)S(1)}, f32[64,2048]{1,0:T(8,128)S(1)}) custom-call(bf16[64,2048]{1,0:T(8,128)(2,1)} %tok_ref.1, f32[688,512]{1,0:T(8,128)} %bitcast.11, f32[688,512]{1,0:T(8,128)} %bitcast.12, f32[688,512]{1,0:T(8,128)} %bitcast.13, ...), custom_call_target="tpu_custom_call" | custom-call | tf_op jit(solution)/shard_map/pallas_call | solution.py:310
  89.0 0.0 copy-done.1
  89.0 0.0 copy-done
  89.0 4.4 %shard_map.103 = (bf16[688,2048]{1,0:T(8,128)(2,1)}, bf16[688,2048]{1,0:T(8,128)(2,1)}, bf16[688,2048]{1,0:T(8,128)(2,1)}, bf16[64,2048]{1,0:T(8,128)(2,1)}) custom-call(bf16[16,688,128]{2,1,0:T(8,128)(2,1)S(1)} %get-tuple-element.12.fg, bf16[16,688,128]{2,1,0:T(8,128)(2,1)S(1)} %get-tuple-element.13.fu, bf16[16,688,128]{2,1,0:T(8,128)(2,1)S(1)} %get-tuple-element.14.fd, ...), custom_call_target="tpu_custom_call" | custom-call | tf_op jit(solution)/shard_map/pallas_call | solution.py:340
Async XLA Ops:
  0.6 88.4 %copy-start.1 = (f32[2048]{0:T(1024)S(1)}, f32[2048]{0:T(1024)}, u32[]{:S(2)}) copy-start(f32[2048]{0:T(1024)} %param.13) | copy-start | bytes 24580
  0.6 88.4 %copy-start = (f32[2048]{0:T(1024)S(1)}, f32[2048]{0:T(1024)}, u32[]{:S(2)}) copy-start(f32[2048]{0:T(1024)} %param.12) | copy-start | bytes 24580

commit v2 on v1

v2 whole, which is shorter than its diff:
```python
import functools

import jax
import jax.numpy as jnp
from jax import lax
from jax.experimental import pallas as pl
from jax.experimental.pallas import tpu as pltpu
from jax.sharding import PartitionSpec as P

MESH = pl.DeviceIdType.MESH
LANES = 128
LAG = 3


def finish(wide, branch, post_gain, post_bias):
    mixed = jnp.sqrt(jnp.float32(2.0)) * wide + 0.5 * branch
    center = jnp.mean(mixed, axis=-1, keepdims=True)
    spread = jnp.mean(jnp.square(mixed - center), axis=-1, keepdims=True)
    return ((mixed - center) * lax.rsqrt(spread + 1e-05) * post_gain + post_bias).astype(
        jnp.bfloat16
    )


def plain(tokens, gate_master, up_master, down_master, norm_gain, post_gain, post_bias):
    row_count = gate_master.shape[0]
    first_row = lax.axis_index("fs") * row_count
    gain_rows = lax.dynamic_slice_in_dim(norm_gain, first_row, row_count, 0)
    gate_piece = (gain_rows[:, None] * gate_master).astype(jnp.bfloat16)
    up_piece = (gain_rows[:, None] * up_master).astype(jnp.bfloat16)
    down_piece = down_master.astype(jnp.bfloat16)
    gate_ready, up_ready, down_ready = (
        lax.all_gather(gate_piece, "fs", axis=0, tiled=True),
        lax.all_gather(up_piece, "fs", axis=0, tiled=True),
        lax.all_gather(down_piece, "fs", axis=0, tiled=True),
    )
    wide = tokens.astype(jnp.float32)
    normed = (wide * lax.rsqrt(jnp.mean(wide * wide, axis=-1, keepdims=True) + 1e-06)).astype(
        jnp.bfloat16
    )
    piece = lax.all_gather(normed, "tp", axis=0, tiled=True)
    gate = jnp.dot(piece, gate_ready, preferred_element_type=jnp.float32)
    upward = jnp.dot(piece, up_ready, preferred_element_type=jnp.float32)
    hidden = (jax.nn.silu(gate) * upward).astype(jnp.bfloat16)
    branch = lax.psum_scatter(
        lax.dot_general(
            hidden, down_ready, (((1,), (1,)), ((), ())), preferred_element_type=jnp.float32
        ).astype(jnp.bfloat16),
        "tp",
        scatter_dimension=0,
        tiled=True,
    ).astype(jnp.float32)
    result = finish(wide, branch, post_gain, post_bias)
    return (gate_ready, up_ready, down_ready, result)


def row_pieces(cols):
    return -(-cols // 32) * 16, cols * 3 // 8 // LANES * LANES


def gather_kernel(
    fs, tp, n, tok_ref, gm_ref, um_ref, dm_ref, gain_ref,
    fg, fu, fd, mixed,
    stage, own, gain, toks, acc_g, acc_u, hid, parts, got,
    up_sem, dn_sem, y_sem, r_sem, ts_sem, tr_sem, ps_sem, pr_sem, i_sem, l_sem,
):
    y, z, t = lax.axis_index("grp"), lax.axis_index("fs"), lax.axis_index("tp")
    cols, rc = gm_ref.shape
    tok_rows, d = tok_ref.shape
    tiles = d // LANES
    middle, split = row_pieces(cols)
    full = (fg, fu, fd)
    masters = (gm_ref, um_ref, dm_ref)
    up_dev = (y, jnp.minimum(z + 1, fs - 1), t)
    dn_dev = (y, jnp.maximum(z - 1, 0), t)
    y_dev = (1 - y, z, t)
    has_up, has_dn = z < fs - 1, z > 0
    at_end = jnp.logical_or(z == 0, z == fs - 1)
    far = fs - 1 - z
    peers = [lax.rem(t + j, tp) for j in range(1, tp)]
    senders = [lax.rem(t + tp - j, tp) for j in range(1, tp)]
    first = [(m, c) for m in (0, 1) for c in range(n)]
    second = [(2, c) for c in range(n)]

    barrier = pltpu.get_barrier_semaphore()

    def greet(dev):
        pl.semaphore_signal(barrier, inc=1, device_id=dev, device_id_type=MESH)

    pl.when(has_up)(lambda: greet(up_dev))
    pl.when(has_dn)(lambda: greet(dn_dev))
    greet(y_dev)
    for peer in peers:
        greet((y, z, peer))

    def pieces(m, c):
        if (m, c) == (2, n - 1):
            return [(0, 0, split), (1, split, cols - split)]
        return [(0, 0, middle), (1, middle, cols - middle)]

    def is_last(m, c, q):
        return (m, c, q[0]) == (2, n - 1, 1)

    def group(m, c, q):
        return m if (m, c) != (2, n - 1) else 3 + q[0]

    def fetch(m, h, c):
        k = h * n + c
        return pltpu.make_async_copy(
            masters[m].at[:, pl.ds(pl.multiple_of(k * LANES, LANES), LANES)],
            stage.at[m, k], i_sem.at[m, k],
        )

    gain_copy = pltpu.make_async_copy(gain_ref, gain, l_sem.at[0])
    tok_fetch = pltpu.make_async_copy(tok_ref, own, l_sem.at[1])
    gain_copy.start()
    for m, c in first:
        fetch(m, y, c).start()
    tok_fetch.start()
    for m, c in second:
        fetch(m, y, c).start()
    for m, c in first + second:
        fetch(m, 1 - y, c).start()

    def tile_of(b, h, c):
        return b * (2 * n) + h * n + c

    def hop(m, c, k, q, dev, sem, skip):
        rows = pl.ds(q[1], q[2])
        slot = (m * (fs - 1) - skip) * (2 * n) + k
        return pltpu.make_async_remote_copy(
            src_ref=full[m].at[k, rows], dst_ref=full[m].at[k, rows],
            send_sem=sem.at[group(m, c, q)], recv_sem=r_sem.at[slot, q[0]],
            device_id=dev, device_id_type=MESH,
        )

    def keep(m, h, c, q):
        if q[0] == 0:
            fetch(m, h, c).wait()
        k = tile_of(z, h, c)
        rows = pl.ds(q[1], q[2])
        v = stage[m, h * n + c, rows, :]
        if m < 2:
            v = v * gain[:, pl.ds(pl.multiple_of(k * LANES, LANES), LANES)]
        full[m][k, rows, :] = v.astype(jnp.bfloat16)

    def send_up(m, h, c, q):
        hop(m, c, tile_of(z, h, c), q, up_dev, up_sem, 0).start()

    def send_dn(m, h, c, q):
        hop(m, c, tile_of(z, h, c), q, dn_dev, dn_sem, 1).start()

    def send_own(m, c, q):
        pl.when(has_up)(lambda: send_up(m, y, c, q))
        pl.when(has_dn)(lambda: send_dn(m, y, c, q))

    def send_end(m, h, c, q):
        pl.when(z == 0)(lambda: send_up(m, h, c, q))
        pl.when(z == fs - 1)(lambda: send_dn(m, h, c, q))

    def part_slot(b, h, c):
        return b * 2 + h if c == 0 else 2 * fs + (c - 1) * 2 + h

    def part_copy(b, h, c, cnt, j, peer):
        k = tile_of(b, h, c)
        return pltpu.make_async_remote_copy(
            src_ref=parts.at[
                pl.ds(k, cnt), pl.ds(pl.multiple_of(peer * tok_rows, tok_rows), tok_rows)
            ],
            dst_ref=got.at[t, pl.ds(k, cnt)],
            send_sem=ps_sem.at[j], recv_sem=pr_sem.at[j, part_slot(b, h, c)],
            device_id=(y, z, peer), device_id_type=MESH,
        )

    def put_parts(ks, part):
        for i, k in enumerate(ks):
            parts[k] = part[:, i * LANES:(i + 1) * LANES].astype(jnp.bfloat16)

    def send_parts(b, h, c, cnt):
        for j, peer in enumerate(peers):
            part_copy(b, h, c, cnt, j, peer).start()

    def product(ks):
        rhs = jnp.concatenate([fd[k] for k in ks], axis=1)
        return jnp.dot(hid[...], rhs, preferred_element_type=jnp.float32)

    def down_half(b, h):
        ks = [tile_of(b, h, c) for c in range(n)]
        put_parts(ks, product(ks))
        send_parts(b, h, 0, n)

    def add_tiles(m, k, start):
        acc = (acc_g, acc_u)[m]
        at = pl.ds(pl.multiple_of(k * LANES, LANES), n * LANES)
        lhs = toks[:, :, at].reshape(tp * tok_rows, n * LANES)
        rhs = jnp.concatenate([full[m][k + i] for i in range(n)], axis=1)
        term = lax.dot_general(
            lhs, rhs, (((1,), (1,)), ((), ())), preferred_element_type=jnp.float32
        )
        acc[...] = term if start else acc[...] + term

    def finish_tiles(b, h, c, cnt):
        k = tile_of(b, h, c)
        for j, peer in enumerate(senders):
            dst = got.at[peer, pl.ds(k, cnt)]
            pltpu.make_async_remote_copy(
                src_ref=dst, dst_ref=dst, send_sem=ps_sem.at[j],
                recv_sem=pr_sem.at[j, part_slot(b, h, c)],
                device_id=(y, z, peer), device_id_type=MESH,
            ).wait_recv()
        mine = pl.ds(pl.multiple_of(t * tok_rows, tok_rows), tok_rows)
        for i in range(cnt):
            branch = parts[k + i, mine, :].astype(jnp.float32)
            for peer in senders:
                branch = branch + got[peer, k + i].astype(jnp.float32)
            at = pl.ds(pl.multiple_of((k + i) * LANES, LANES), LANES)
            wide = own[:, at].astype(jnp.float32)
            mixed[:, at] = jnp.sqrt(jnp.float32(2.0)) * wide + 0.5 * branch

    def ends(p):
        low, high = z - 1 - p, z + 1 + p
        return ((low, low >= 0, low == 0), (high, high <= fs - 1, high == fs - 1))

    sums, downs, fins = [], [], []

    def work(todo, count):
        for _ in range(min(count, len(todo))):
            ok, item = todo.pop(0)
            if ok is None:
                item()
            else:
                pl.when(ok)(item)

    def arrived(m, c, q, p):
        (low, has_low, low_end), (high, has_high, high_end) = ends(p)
        straight = p == 0 or is_last(m, c, q)

        def take(b, b_end, more, dev, sem, skip):
            k = tile_of(b, y, c)
            hop(m, c, k, q, dev, sem, skip).wait_recv()
            pl.when(more)(lambda: hop(m, c, k, q, dev, sem, skip).start())
            cross = lambda: hop(m, c, k, q, y_dev, y_sem, skip).start()
            if straight:
                pl.when(jnp.logical_not(b_end))(cross)
            else:
                cross()

        pl.when(has_low)(lambda: take(low, low_end, has_up, up_dev, up_sem, 0))
        pl.when(has_high)(lambda: take(high, high_end, has_dn, dn_dev, dn_sem, 1))

    def doubled(c, q, p):
        (low, has_low, low_end), (high, has_high, high_end) = ends(p)

        def take(b, more, dev, sem, skip):
            k = tile_of(b, 1 - y, c)
            hop(2, c, k, q, dev, sem, skip).wait_recv()
            pl.when(more)(lambda: hop(2, c, k, q, dev, sem, skip).start())

        pl.when(jnp.logical_and(has_low, low_end))(lambda: take(low, has_up, up_dev, up_sem, 0))
        pl.when(jnp.logical_and(has_high, high_end))(lambda: take(high, has_dn, dn_dev, dn_sem, 1))

    def crossed(m, c, p):
        for skip, (b, ok, b_end) in enumerate(ends(p)):
            k = tile_of(b, 1 - y, c)
            for q in pieces(m, c):
                here = jnp.logical_and(ok, jnp.logical_not(b_end)) if is_last(m, c, q) else ok
                pl.when(here)(
                    lambda k=k, q=q, skip=skip: hop(m, c, k, q, y_dev, y_sem, skip).wait_recv()
                )

    def later(m, c, p, h):
        if c < n - 1:
            return
        for b, ok, _ in ends(p):
            if m == 2:
                downs.append((ok, lambda b=b: down_half(b, h)))
                fins.append((ok, lambda b=b: finish_tiles(b, h, 0, n)))
            else:
                sums.append((ok, lambda b=b: add_tiles(m, tile_of(b, h, 0), False)))

    def tok_copy(j, peer, origin):
        return pltpu.make_async_remote_copy(
            src_ref=toks.at[origin], dst_ref=toks.at[origin],
            send_sem=ts_sem.at[j], recv_sem=tr_sem.at[j],
            device_id=(y, z, peer), device_id_type=MESH,
        )

    plan = [(m, c, q) for m, c in first for q in pieces(m, c)]
    gain_copy.wait()
    keep(plan[0][0], y, *plan[0][1:])
    expected = has_up.astype(jnp.int32) + has_dn.astype(jnp.int32) + tp
    pl.semaphore_wait(barrier, expected)
    for before, after in zip(plan, plan[1:]):
        keep(after[0], y, *after[1:])
        send_own(*before)
    tok_fetch.wait()
    wide = own[...].astype(jnp.float32)
    scale = lax.rsqrt(jnp.mean(wide * wide, axis=-1, keepdims=True) + 1e-06)
    send_own(*plan[-1])
    toks[t] = (wide * scale).astype(jnp.bfloat16)
    late = [(m, c, q) for m, c in second for q in pieces(m, c)]
    for m, c, q in late:
        keep(m, y, c, q)
    for j, peer in enumerate(peers):
        tok_copy(j, peer, t).start()
    for m, c, q in plan:
        keep(m, 1 - y, c, q)
    for m, c, q in plan:
        send_end(m, 1 - y, c, q)
    for m, c, q in late:
        send_end(m, y, c, q)
    for m, c, q in late:
        keep(m, 1 - y, c, q)
    for m, c, q in late:
        send_end(m, 1 - y, c, q)

    waiting = []

    def settle(count):
        while len(waiting) > count:
            m, c, p = waiting.pop(0)
            crossed(m, c, p)
            later(m, c, p, 1 - y)

    for p in range(fs - 1):
        for m, c in first:
            for q in pieces(m, c):
                arrived(m, c, q, p)
            later(m, c, p, y)
            waiting.append((m, c, p))
            settle(LAG)
            if p > 0:
                work(sums, 4)
        if p == 0:
            for j, peer in enumerate(senders):
                tok_copy(j, peer, peer).wait_recv()
            sums[:0] = [
                (None, lambda m=m, h=h: add_tiles(m, tile_of(z, h, 0), h == 0))
                for m in (0, 1) for h in (0, 1)
            ]

    @pl.when(jnp.logical_not(at_end))
    def _():
        for m, c, q in late:
            send_own(m, c, q)

    for p in range(fs - 2):
        for m, c in second:
            for q in pieces(m, c):
                arrived(m, c, q, p)
                if is_last(m, c, q):
                    doubled(c, q, p)
            if p == 0 and c == 0:
                settle(0)
                work(sums, len(sums))
                hid[...] = (jax.nn.silu(acc_g[...]) * acc_u[...]).astype(jnp.bfloat16)
                for h in (0, 1):
                    downs.append((None, lambda h=h: down_half(z, h)))
                    fins.append((None, lambda h=h: finish_tiles(z, h, 0, n)))
            later(m, c, p, y)
            waiting.append((m, c, p))
            settle(1)
            work(downs, 4)

    def far_tile(h, c):
        return tile_of(far, h, c)

    far_skip = (far > z).astype(jnp.int32)

    def far_take(c, q):
        k = far_tile(y, c)
        hop(2, c, k, q, y_dev, y_sem, far_skip).wait_recv()
        if not is_last(2, c, q):
            hop(2, c, k, q, y_dev, y_sem, far_skip).start()

    def far_cross(c, q):
        hop(2, c, far_tile(1 - y, c), q, y_dev, y_sem, far_skip).wait_recv()

    def far_down(c):
        ks = [far_tile(h, c) for h in (0, 1)]
        put_parts(ks, product(ks))
        for h in (0, 1):
            send_parts(far, h, c, 1)

    head = [(c, q) for _, c, q in late if c < n - 1]
    tail = [q for _, c, q in late if c == n - 1]

    @pl.when(at_end)
    def _():
        for c, q in head:
            far_take(c, q)

    settle(0)
    work(downs, len(downs))
    pl.when(at_end)(lambda: far_take(n - 1, tail[0]))
    work(fins, 4)

    @pl.when(at_end)
    def _():
        for c, q in head:
            far_cross(c, q)
        for c in range(n - 1):
            far_down(c)

    work(fins, len(fins))

    @pl.when(at_end)
    def _():
        far_take(n - 1, tail[1])
        far_cross(n - 1, tail[1])
        far_cross(n - 1, tail[0])
        far_down(n - 1)
        for c in range(n):
            for h in (0, 1):
                finish_tiles(far, h, c, 1)

    def sent(g, count, sem, dev):
        if count:
            rows = slice(0, cols) if g < 3 else slice(0, split) if g == 3 else slice(split, cols)
            ref = full[min(g, 2)].at[pl.ds(0, count), rows]
            pltpu.make_async_remote_copy(
                src_ref=ref, dst_ref=ref, send_sem=sem.at[g], recv_sem=r_sem.at[0, 0],
                device_id=dev, device_id_type=MESH,
            ).wait_send()

    def sends(j, g):
        base = (n, n, n - 1, 1, 1)[g]
        outer = (0, fs - 1)
        twice = lambda b: 2 * base if g == 4 and b in outer else base
        mine = 2 * base if j in outer else base
        up = mine + sum(twice(b) for b in range(j)) if j < fs - 1 else 0
        dn = mine + sum(twice(b) for b in range(j + 1, fs)) if j > 0 else 0
        cross = sum(
            base for b in range(fs)
            if b != j and not (b in outer and (abs(b - j) == 1 or g == 4))
        )
        return up, dn, cross

    for j in range(fs):
        @pl.when(z == j)
        def _(j=j):
            for g in range(5):
                up, dn, cross = sends(j, g)
                sent(g, up, up_sem, up_dev)
                sent(g, dn, dn_sem, dn_dev)
                sent(g, cross, y_sem, y_dev)

    for j, peer in enumerate(peers):
        tok_copy(j, peer, t).wait_send()
        ref = parts.at[:, pl.ds(0, tok_rows)]
        pltpu.make_async_remote_copy(
            src_ref=ref, dst_ref=ref, send_sem=ps_sem.at[j], recv_sem=pr_sem.at[j, 0],
            device_id=(y, z, peer), device_id_type=MESH,
        ).wait_send()


def emit_kernel(
    fg, fu, fd, mixed, pg_ref, pb_ref, go_ref, uo_ref, do_ref, res_ref, res, sem, res_sem
):
    tiles = fg.shape[0]
    copies = [
        pltpu.make_async_copy(src.at[k], out.at[:, k * LANES:(k + 1) * LANES], sem.at[m, k])
        for m, (src, out) in enumerate(((fg, go_ref), (fu, uo_ref), (fd, do_ref)))
        for k in range(tiles)
    ]
    for copy in copies:
        copy.start()
    mix = mixed[...]
    center = jnp.mean(mix, axis=-1, keepdims=True)
    off = mix - center
    spread = jnp.mean(jnp.square(off), axis=-1, keepdims=True)
    res[...] = (
        off * lax.rsqrt(spread + 1e-05) * pg_ref[...] + pb_ref[...]
    ).astype(jnp.bfloat16)
    put = pltpu.make_async_copy(res, res_ref, res_sem)
    put.start()
    for copy in copies:
        copy.wait()
    put.wait()


def fused(fs, tp, n, tokens, gate_master, up_master, down_master, norm_gain, post_gain, post_bias):
    rc, cols = gate_master.shape
    tok_rows, d = tokens.shape
    tiles, rows = d // LANES, tp * tok_rows
    bf, f32 = jnp.bfloat16, jnp.float32
    held = pltpu.VMEM((tiles, cols, LANES), bf)
    vmem = pl.BlockSpec(memory_space=pltpu.VMEM)
    anywhere = pl.BlockSpec(memory_space=pl.ANY)
    dma = pltpu.SemaphoreType.DMA
    sources = (tokens, gate_master.T, up_master.T, down_master.T, norm_gain[None, :])
    kept = pl.pallas_call(
        functools.partial(gather_kernel, fs, tp, n),
        out_shape=(held, held, held, pltpu.VMEM((tok_rows, d), f32)),
        in_specs=[anywhere] * 5,
        out_specs=(vmem,) * 4,
        scratch_shapes=[
            pltpu.VMEM((3, 2 * n, cols, LANES), f32),
            pltpu.VMEM((tok_rows, d), bf),
            pltpu.VMEM((1, d), f32),
            pltpu.VMEM((tp, tok_rows, d), bf),
            pltpu.VMEM((rows, cols), f32),
            pltpu.VMEM((rows, cols), f32),
            pltpu.VMEM((rows, cols), bf),
            pltpu.VMEM((tiles, rows, LANES), bf),
            pltpu.VMEM((tp, tiles, tok_rows, LANES), bf),
            dma((5,)), dma((5,)), dma((5,)), dma((3 * (fs - 1) * 2 * n, 2)),
            dma((tp - 1,)), dma((tp - 1,)), dma((tp - 1,)), dma((tp - 1, 2 * (fs + n - 1))),
            dma((3, 2 * n)), dma((2,)),
        ],
        compiler_params=pltpu.CompilerParams(
            collective_id=0, has_side_effects=True, vmem_limit_bytes=50 * 2**20
        ),
    )(*(pltpu.with_memory_space_constraint(x, pltpu.HBM) for x in sources))
    ready = jax.ShapeDtypeStruct((cols, d), bf)
    gate, up, down, result = pl.pallas_call(
        emit_kernel,
        out_shape=(ready, ready, ready, jax.ShapeDtypeStruct((tok_rows, d), bf)),
        in_specs=[vmem] * 6,
        out_specs=(anywhere,) * 4,
        scratch_shapes=[
            pltpu.VMEM((tok_rows, d), bf), dma((3, tiles)), pltpu.SemaphoreType.DMA,
        ],
        compiler_params=pltpu.CompilerParams(vmem_limit_bytes=20 * 2**20),
    )(
        *(pltpu.with_memory_space_constraint(x, pltpu.VMEM) for x in kept),
        post_gain[None, :], post_bias[None, :],
    )
    return gate.T, up.T, down.T, result


def solution(mesh):
    grp, fs, tp = mesh.shape["grp"], mesh.shape["fs"], mesh.shape["tp"]

    def local(tokens, gate_master, *rest):
        rc, cols = gate_master.shape
        n = rc // (2 * LANES)
        fits = grp == 2 and fs > 2 and rc % (2 * LANES) == 0 and 2 * n * fs <= 32
        fits = fits and cols % 16 == 0 and tokens.shape[0] % 16 == 0
        middle, split = row_pieces(cols)
        fits = fits and 0 < middle < cols and 0 < split < cols
        if fits:
            return fused(fs, tp, n, tokens, gate_master, *rest)
        return plain(tokens, gate_master, *rest)

    return jax.shard_map(
        local,
        mesh=mesh,
        in_specs=(
            P(("grp", "fs", "tp"), None),
            P("fs", "tp"),
            P("fs", "tp"),
            P("fs", "tp"),
            P(),
            P(),
            P(),
        ),
        out_specs=(P("grp", "tp"), P("grp", "tp"), P("grp", "tp"), P(("grp", "fs", "tp"), None)),
        check_vma=False,
    )
```

time: 93.6 us -> 85.9 us (0.918)
  Pallas kernels: 92.8 us -> 85 us
    pallas_call x1, Pallas kernels: 88.3 us -> 81.2 us  [fused(): pl.pallas_call(functools.partial(gather_kernel, fs, tp, n), out_shape=(he...]
where the time goes in v2:
time: 85.9 us; the launch traced here: 85.7 us
  Pallas kernels  85 us (99%)
    pallas_call x1, Pallas kernels, fused(): pl.pallas_call(functools.partial(gather_kernel, fs, tp, n), out_shape=(he...  81.2 us
    pallas_call x1, Pallas kernels, fused(): pl.pallas_call(emit_kernel, out_shape=(ready, ready, ready, jax.ShapeDtyp...  3.81 us

profile of v2, /device:TPU:0, one launch (start us, length us, event | category | flops | bytes accessed | tf_op | source)
XLA Modules:
  0.0 85.7 jit_solution(13562157521769547898)
XLA Ops:
  0.6 0.0 copy-start.1
  0.6 0.0 copy-start
  0.7 81.2 %shard_map.102 = (bf16[16,688,128]{2,1,0:T(8,128)(2,1)S(1)}, bf16[16,688,128]{2,1,0:T(8,128)(2,1)S(1)}, bf16[16,688,128]{2,1,0:T(8,128)(2,1)S(1)}, f32[64,2048]{1,0:T(8,128)S(1)}) custom-call(bf16[64,2048]{1,0:T(8,128)(2,1)} %tok_ref.1, f32[688,512]{1,0:T(8,128)} %bitcast.11, f32[688,512]{1,0:T(8,128)} %bitcast.12, f32[688,512]{1,0:T(8,128)} %bitcast.13, ...), custom_call_target="tpu_custom_call" | custom-call | tf_op jit(solution)/shard_map/pallas_call | solution.py:491
  81.9 0.0 copy-done.1
  81.9 0.0 copy-done
  81.9 3.8 %shard_map.103 = (bf16[688,2048]{1,0:T(8,128)(2,1)}, bf16[688,2048]{1,0:T(8,128)(2,1)}, bf16[688,2048]{1,0:T(8,128)(2,1)}, bf16[64,2048]{1,0:T(8,128)(2,1)}) custom-call(bf16[16,688,128]{2,1,0:T(8,128)(2,1)S(1)} %get-tuple-element.12.fg, bf16[16,688,128]{2,1,0:T(8,128)(2,1)S(1)} %get-tuple-element.13.fu, bf16[16,688,128]{2,1,0:T(8,128)(2,1)S(1)} %get-tuple-element.14.fd, ...), custom_call_target="tpu_custom_call" | custom-call | tf_op jit(solution)/shard_map/pallas_call | solution.py:515
Async XLA Ops:
  0.6 81.3 %copy-start.1 = (f32[2048]{0:T(1024)S(1)}, f32[2048]{0:T(1024)}, u32[]{:S(2)}) copy-start(f32[2048]{0:T(1024)} %param.13) | copy-start | bytes 24580
  0.6 81.3 %copy-start = (f32[2048]{0:T(1024)S(1)}, f32[2048]{0:T(1024)}, u32[]{:S(2)}) copy-start(f32[2048]{0:T(1024)} %param.12) | copy-start | bytes 24580

commit v3 on v2

v3 whole, which is shorter than its diff:
```python
import functools

import jax
import jax.numpy as jnp
from jax import lax
from jax.experimental import pallas as pl
from jax.experimental.pallas import tpu as pltpu
from jax.sharding import PartitionSpec as P

MESH = pl.DeviceIdType.MESH
LANES = 128
LAG = 3


def finish(wide, branch, post_gain, post_bias):
    mixed = jnp.sqrt(jnp.float32(2.0)) * wide + 0.5 * branch
    center = jnp.mean(mixed, axis=-1, keepdims=True)
    spread = jnp.mean(jnp.square(mixed - center), axis=-1, keepdims=True)
    return ((mixed - center) * lax.rsqrt(spread + 1e-05) * post_gain + post_bias).astype(
        jnp.bfloat16
    )


def plain(tokens, gate_master, up_master, down_master, norm_gain, post_gain, post_bias):
    row_count = gate_master.shape[0]
    first_row = lax.axis_index("fs") * row_count
    gain_rows = lax.dynamic_slice_in_dim(norm_gain, first_row, row_count, 0)
    gate_piece = (gain_rows[:, None] * gate_master).astype(jnp.bfloat16)
    up_piece = (gain_rows[:, None] * up_master).astype(jnp.bfloat16)
    down_piece = down_master.astype(jnp.bfloat16)
    gate_ready, up_ready, down_ready = (
        lax.all_gather(gate_piece, "fs", axis=0, tiled=True),
        lax.all_gather(up_piece, "fs", axis=0, tiled=True),
        lax.all_gather(down_piece, "fs", axis=0, tiled=True),
    )
    wide = tokens.astype(jnp.float32)
    normed = (wide * lax.rsqrt(jnp.mean(wide * wide, axis=-1, keepdims=True) + 1e-06)).astype(
        jnp.bfloat16
    )
    piece = lax.all_gather(normed, "tp", axis=0, tiled=True)
    gate = jnp.dot(piece, gate_ready, preferred_element_type=jnp.float32)
    upward = jnp.dot(piece, up_ready, preferred_element_type=jnp.float32)
    hidden = (jax.nn.silu(gate) * upward).astype(jnp.bfloat16)
    branch = lax.psum_scatter(
        lax.dot_general(
            hidden, down_ready, (((1,), (1,)), ((), ())), preferred_element_type=jnp.float32
        ).astype(jnp.bfloat16),
        "tp",
        scatter_dimension=0,
        tiled=True,
    ).astype(jnp.float32)
    result = finish(wide, branch, post_gain, post_bias)
    return (gate_ready, up_ready, down_ready, result)


def gather_kernel(
    fs, tp, n, tok_ref, gm_ref, um_ref, dm_ref, gain_ref,
    fg, fu, fd, mixed,
    stage, own, gain, toks, acc_g, acc_u, hid, parts, got,
    hid_far, parts_far, got_far, sum_far, branch_far,
    up_sem, dn_sem, y_sem, r_sem, x_sem, t_sem, ps_sem, pr_sem, i_sem, l_sem, h_sem, p_sem, b_sem,
):
    y, z, t = lax.axis_index("grp"), lax.axis_index("fs"), lax.axis_index("tp")
    cols, rc = gm_ref.shape
    tok_rows, d = tok_ref.shape
    tiles = d // LANES
    middle = -(-cols // 32) * 16
    pieces = ((0, 0, middle), (1, middle, cols - middle))
    full = (fg, fu, fd)
    masters = (gm_ref, um_ref, dm_ref)
    up_dev = (y, jnp.minimum(z + 1, fs - 1), t)
    dn_dev = (y, jnp.maximum(z - 1, 0), t)
    y_dev = (1 - y, z, t)
    has_up, has_dn = z < fs - 1, z > 0
    at_end = jnp.logical_or(z == 0, z == fs - 1)
    by_end = jnp.logical_or(z == 1, z == fs - 2)
    far = jnp.where(z < 2, fs - 1, 0)
    cross = 1 - y
    end_dev = (y, jnp.where(z == 1, 0, fs - 1), t)
    helper = (y, jnp.where(z == 0, 1, fs - 2), t)
    peers = [lax.rem(t + j, tp) for j in range(1, tp)]
    senders = [lax.rem(t + tp - j, tp) for j in range(1, tp)]
    first = [(m, c) for m in (0, 1) for c in range(n)]
    second = [(2, c) for c in range(n)]

    barrier = pltpu.get_barrier_semaphore()

    def greet(dev):
        pl.semaphore_signal(barrier, inc=1, device_id=dev, device_id_type=MESH)

    pl.when(has_up)(lambda: greet(up_dev))
    pl.when(has_dn)(lambda: greet(dn_dev))
    greet(y_dev)
    for peer in peers:
        greet((y, z, peer))

    def is_last(m, c, q):
        return (m, c, q[0]) == (2, n - 1, 1)

    def group(m, c, q):
        return m if (m, c) != (2, n - 1) else 3 + q[0]

    def fetch(m, h, c, slot):
        k = h * n + c
        return pltpu.make_async_copy(
            masters[m].at[:, pl.ds(pl.multiple_of(k * LANES, LANES), LANES)],
            stage.at[m, k], i_sem.at[slot],
        )

    def fetched(m, h, c):
        if h is not y:
            if (m, c) == first[0]:
                ref = stage.at[:, pl.ds(h * n, n)]
                pltpu.make_async_copy(ref, ref, i_sem.at[2 * n + 1]).wait()
        elif m == 2:
            if c == 0:
                ref = stage.at[2, pl.ds(h * n, n)]
                pltpu.make_async_copy(ref, ref, i_sem.at[2 * n]).wait()
        else:
            fetch(m, h, c, m * n + c).wait()

    gain_copy = pltpu.make_async_copy(gain_ref, gain, l_sem.at[0])
    tok_fetch = pltpu.make_async_copy(tok_ref, own, l_sem.at[1])
    gain_copy.start()
    fetch(first[0][0], y, first[0][1], 0).start()

    def tile_of(b, h, c):
        return b * (2 * n) + h * n + c

    def hop(m, c, k, q, dev, sem, skip, other=False):
        rows = pl.ds(q[1], q[2])
        b = k // (2 * n)
        if other:
            recv_sem = x_sem.at[b - skip, group(m, c, q)]
        else:
            recv_sem = r_sem.at[(m * (fs - 1) + b - skip) * n + c, q[0]]
        return pltpu.make_async_remote_copy(
            src_ref=full[m].at[k, rows], dst_ref=full[m].at[k, rows],
            send_sem=sem.at[group(m, c, q)], recv_sem=recv_sem,
            device_id=dev, device_id_type=MESH,
        )

    def crossed_all(m, b, g, skip):
        k = tile_of(b, cross, 0)
        if g < 3:
            ref = full[m].at[pl.ds(k, (n, n, n - 1)[g])]
        else:
            q = pieces[g - 3]
            ref = full[2].at[k + n - 1, pl.ds(q[1], q[2])]
        pltpu.make_async_remote_copy(
            src_ref=ref, dst_ref=ref, send_sem=y_sem.at[g], recv_sem=x_sem.at[b - skip, g],
            device_id=y_dev, device_id_type=MESH,
        ).wait_recv()

    def keep(m, h, c, q):
        if q[0] == 0:
            fetched(m, h, c)
        k = tile_of(z, h, c)
        rows = pl.ds(q[1], q[2])
        v = stage[m, h * n + c, rows, :]
        if m < 2:
            v = v * gain[:, pl.ds(pl.multiple_of(k * LANES, LANES), LANES)]
        full[m][k, rows, :] = v.astype(jnp.bfloat16)

    def send_up(m, h, c, q):
        hop(m, c, tile_of(z, h, c), q, up_dev, up_sem, 0, h is not y).start()

    def send_dn(m, h, c, q):
        hop(m, c, tile_of(z, h, c), q, dn_dev, dn_sem, 1, h is not y).start()

    def part_copy(b, h, j, peer):
        k = tile_of(b, h, 0)
        return pltpu.make_async_remote_copy(
            src_ref=parts.at[
                pl.ds(k, n), pl.ds(pl.multiple_of(peer * tok_rows, tok_rows), tok_rows)
            ],
            dst_ref=got.at[t, pl.ds(k, n)],
            send_sem=ps_sem.at[0], recv_sem=pr_sem.at[b],
            device_id=(y, z, peer), device_id_type=MESH,
        )

    def product(lhs, k, to, at):
        rhs = jnp.concatenate([fd[k + i] for i in range(n)], axis=1)
        part = jnp.dot(lhs[...], rhs, preferred_element_type=jnp.float32)
        for i in range(n):
            to[at + i] = part[:, i * LANES:(i + 1) * LANES].astype(jnp.bfloat16)

    def down_half(b, h):
        k = tile_of(b, h, 0)
        product(hid, k, parts, k)
        for j, peer in enumerate(peers):
            part_copy(b, h, j, peer).start()

    def add_tiles(m, k, start):
        acc = (acc_g, acc_u)[m]
        at = pl.ds(pl.multiple_of(k * LANES, LANES), n * LANES)
        lhs = toks[:, :, at].reshape(tp * tok_rows, n * LANES)
        rhs = jnp.concatenate([full[m][k + i] for i in range(n)], axis=1)
        term = lax.dot_general(
            lhs, rhs, (((1,), (1,)), ((), ())), preferred_element_type=jnp.float32
        )
        acc[...] = term if start else acc[...] + term

    mine = pl.ds(pl.multiple_of(t * tok_rows, tok_rows), tok_rows)

    def mix(k, branch):
        at = pl.ds(pl.multiple_of(k * LANES, LANES), LANES)
        wide = own[:, at].astype(jnp.float32)
        mixed[:, at] = jnp.sqrt(jnp.float32(2.0)) * wide + 0.5 * branch

    def finish_origin(b):
        k = tile_of(b, 0, 0)
        ref = got.at[pl.ds(0, tp - 1), pl.ds(k, 2 * n)]
        pltpu.make_async_remote_copy(
            src_ref=ref, dst_ref=ref, send_sem=ps_sem.at[0], recv_sem=pr_sem.at[b],
            device_id=y_dev, device_id_type=MESH,
        ).wait_recv()
        for i in range(2 * n):
            branch = parts[k + i, mine, :].astype(jnp.float32)
            for peer in senders:
                branch = branch + got[peer, k + i].astype(jnp.float32)
            mix(k + i, branch)

    hid_copy = pltpu.make_async_remote_copy(
        src_ref=hid, dst_ref=hid_far, send_sem=h_sem.at[0], recv_sem=h_sem.at[1],
        device_id=helper, device_id_type=MESH,
    )
    sum_copy = pltpu.make_async_remote_copy(
        src_ref=sum_far, dst_ref=branch_far, send_sem=b_sem.at[0], recv_sem=b_sem.at[1],
        device_id=end_dev, device_id_type=MESH,
    )

    def far_copy(j, peer):
        return pltpu.make_async_remote_copy(
            src_ref=parts_far.at[
                :, pl.ds(pl.multiple_of(peer * tok_rows, tok_rows), tok_rows)
            ],
            dst_ref=got_far.at[j], send_sem=p_sem.at[0], recv_sem=p_sem.at[1],
            device_id=(y, z, peer), device_id_type=MESH,
        )

    def help_down():
        hid_copy.wait_recv()
        for h in (0, 1):
            product(hid_far, tile_of(far, h, 0), parts_far, h * n)
        for j, peer in enumerate(peers):
            far_copy(j, peer).start()

    def help_sum():
        pltpu.make_async_remote_copy(
            src_ref=got_far, dst_ref=got_far, send_sem=p_sem.at[0], recv_sem=p_sem.at[1],
            device_id=y_dev, device_id_type=MESH,
        ).wait_recv()
        total = parts_far[:, mine, :].astype(jnp.float32)
        for j in range(tp - 1):
            total = total + got_far[j].astype(jnp.float32)
        sum_far[...] = total.astype(jnp.bfloat16)
        sum_copy.start()

    def ends(p):
        low, high = z - 1 - p, z + 1 + p
        return ((low, low >= 0, low == 0), (high, high <= fs - 1, high == fs - 1))

    sums, downs, fins = [], [], []

    def work(todo, count):
        for _ in range(min(count, len(todo))):
            ok, item = todo.pop(0)
            if ok is None:
                item()
            else:
                pl.when(ok)(item)

    def take(m, c, q, b, b_end, more, dev, sem, skip, straight):
        k = tile_of(b, y, c)
        hop(m, c, k, q, dev, sem, skip).wait_recv()
        pl.when(more)(lambda: hop(m, c, k, q, dev, sem, skip).start())
        pass_on = lambda: hop(m, c, k, q, y_dev, y_sem, skip, True).start()
        if straight:
            pl.when(jnp.logical_not(b_end))(pass_on)
        else:
            pass_on()

    def arrived_dn(m, c, q, p):
        _, (high, ok, b_end) = ends(p)
        straight = p == 0 or is_last(m, c, q)
        pl.when(ok)(lambda: take(m, c, q, high, b_end, has_dn, dn_dev, dn_sem, 1, straight))

    def arrived_up(m, c, q, p):
        (low, ok, b_end), _ = ends(p)
        straight = p == 0 or is_last(m, c, q)
        pl.when(ok)(lambda: take(m, c, q, low, b_end, has_up, up_dev, up_sem, 0, straight))

    def arrived(m, c, q, p):
        arrived_dn(m, c, q, p)
        arrived_up(m, c, q, p)

    def doubled(c, q, p):
        def take_other(b, more, dev, sem, skip):
            crossed_all(2, b, 4, skip)
            k = tile_of(b, cross, c)
            pl.when(more)(lambda: hop(2, c, k, q, dev, sem, skip, True).start())

        (low, has_low, low_end), (high, has_high, high_end) = ends(p)
        pl.when(jnp.logical_and(has_high, high_end))(
            lambda: take_other(high, has_dn, dn_dev, dn_sem, 1)
        )
        pl.when(jnp.logical_and(has_low, low_end))(
            lambda: take_other(low, has_up, up_dev, up_sem, 0)
        )

    def crossed(m, c, p):
        groups = {n - 1: (m,) if m < 2 else (3, 4), n - 2: () if m < 2 else (2,)}.get(c, ())
        for skip, (b, ok, b_end) in enumerate(ends(p)):
            for g in groups:
                here = jnp.logical_and(ok, jnp.logical_not(b_end)) if g == 4 else ok
                pl.when(here)(lambda b=b, g=g, skip=skip: crossed_all(m, b, g, skip))

    def later(m, c, p, h):
        if c < n - 1:
            return
        for b, ok, _ in ends(p):
            if m == 2:
                downs.append((ok, lambda b=b: down_half(b, h)))
                if h is not y:
                    fins.append((ok, lambda b=b: finish_origin(b)))
            else:
                sums.append((ok, lambda b=b: add_tiles(m, tile_of(b, h, 0), False)))

    def tok_copy(peer, origin):
        return pltpu.make_async_remote_copy(
            src_ref=toks.at[origin], dst_ref=toks.at[origin],
            send_sem=t_sem.at[0], recv_sem=t_sem.at[1],
            device_id=(y, z, peer), device_id_type=MESH,
        )

    plan = [(m, c, q) for m, c in first for q in pieces]
    gain_copy.wait()
    keep(plan[0][0], y, *plan[0][1:])
    for m, c in first[1:]:
        fetch(m, y, c, m * n + c).start()
    tok_fetch.start()
    for m, c in second:
        fetch(m, y, c, 2 * n).start()
    for m, c in first + second:
        fetch(m, cross, c, 2 * n + 1).start()
    pl.semaphore_wait(barrier, has_up.astype(jnp.int32) + has_dn.astype(jnp.int32) + tp)
    tok_all = pltpu.make_async_remote_copy(
        src_ref=toks.at[pl.ds(0, tp - 1)], dst_ref=toks.at[pl.ds(0, tp - 1)],
        send_sem=t_sem.at[0], recv_sem=t_sem.at[1], device_id=y_dev, device_id_type=MESH,
    )
    late = [(m, c, q) for m, c in second for q in pieces]

    def send_own(m, c, q):
        pl.when(has_dn)(lambda: send_dn(m, y, c, q))
        pl.when(has_up)(lambda: send_up(m, y, c, q))

    for before, after in zip(plan, plan[1:]):
        keep(after[0], y, *after[1:])
        send_own(*before)
    tok_fetch.wait()
    wide = own[...].astype(jnp.float32)
    scale = lax.rsqrt(jnp.mean(wide * wide, axis=-1, keepdims=True) + 1e-06)
    send_own(*plan[-1])
    toks[t] = (wide * scale).astype(jnp.bfloat16)
    for m, c, q in late:
        keep(m, y, c, q)
    for peer in peers:
        tok_copy(peer, t).start()
    for m, c, q in plan + late:
        keep(m, cross, c, q)
    order = [(m, cross, c, q) for m, c, q in plan]
    order += [(m, y, c, q) for m, c, q in late]
    order += [(m, cross, c, q) for m, c, q in late]

    @pl.when(z == fs - 1)
    def _():
        for item in order:
            send_dn(*item)

    @pl.when(z == 0)
    def _():
        for item in order:
            send_up(*item)

    waiting = []

    def settle(count):
        while len(waiting) > count:
            m, c, p = waiting.pop(0)
            crossed(m, c, p)
            later(m, c, p, cross)

    for p in range(fs - 1):
        for m, c in first:
            for q in pieces:
                arrived(m, c, q, p)
            later(m, c, p, y)
            waiting.append((m, c, p))
            settle(LAG)
            if p > 0:
                work(sums, 4)
        if p == 0:
            tok_all.wait_recv()
            sums[:0] = [
                (None, lambda m=m, h=h: add_tiles(m, tile_of(z, h, 0), h == 0))
                for m in (0, 1) for h in (0, 1)
            ]

    @pl.when(jnp.logical_not(at_end))
    def _():
        for m, c, q in late:
            send_own(m, c, q)

    for p in range(fs - 2):
        for m, c in second:
            for q in pieces:
                arrived(m, c, q, p)
                if is_last(m, c, q):
                    doubled(c, q, p)
            if p == 0 and c == 0:
                settle(0)
                work(sums, len(sums))
                hid[...] = (jax.nn.silu(acc_g[...]) * acc_u[...]).astype(jnp.bfloat16)
                pl.when(at_end)(hid_copy.start)
                for h in (0, 1):
                    downs.append((None, lambda h=h: down_half(z, h)))
                fins.append((None, lambda: finish_origin(z)))
            later(m, c, p, y)
            waiting.append((m, c, p))
            settle(1)
            work(downs, 4)

    def far_tile(h, c):
        return tile_of(far, h, c)

    far_skip = (far > z).astype(jnp.int32)

    def far_take(c, q):
        k = far_tile(y, c)
        hop(2, c, k, q, y_dev, y_sem, far_skip).wait_recv()
        if not is_last(2, c, q):
            hop(2, c, k, q, y_dev, y_sem, far_skip, True).start()

    @pl.when(at_end)
    def _():
        for _, c, q in late[:-1]:
            far_take(c, q)

    settle(0)
    work(downs, len(downs))
    pl.when(by_end)(help_down)
    work(fins, len(fins))
    pl.when(by_end)(help_sum)

    @pl.when(at_end)
    def _():
        far_take(*late[-1][1:])
        for g in (2, 3, 4) if n > 1 else (3, 4):
            crossed_all(2, far, g, far_skip)
        sum_copy.wait_recv()
        for i in range(2 * n):
            mix(far * (2 * n) + i, branch_far[i].astype(jnp.float32))

    def sent(g, count, sem, dev):
        if count:
            rows = (slice(0, cols),) * 3 + (slice(0, middle), slice(middle, cols))
            rows = rows[g]
            ref = full[min(g, 2)].at[pl.ds(0, count), rows]
            pltpu.make_async_remote_copy(
                src_ref=ref, dst_ref=ref, send_sem=sem.at[g], recv_sem=b_sem.at[1],
                device_id=dev, device_id_type=MESH,
            ).wait_send()

    def sends(j, g):
        base = (n, n, n - 1, 1, 1)[g]
        outer = (0, fs - 1)
        twice = lambda b: 2 * base if g == 4 and b in outer else base
        mine = 2 * base if j in outer else base
        up = mine + sum(twice(b) for b in range(j)) if j < fs - 1 else 0
        dn = mine + sum(twice(b) for b in range(j + 1, fs)) if j > 0 else 0
        cross = sum(
            base for b in range(fs)
            if b != j and not (b in outer and (abs(b - j) == 1 or g == 4))
        )
        return up, dn, cross

    for j in range(fs):
        @pl.when(z == j)
        def _(j=j):
            for g in range(5):
                up, dn, cross = sends(j, g)
                sent(g, up, up_sem, up_dev)
                sent(g, dn, dn_sem, dn_dev)
                sent(g, cross, y_sem, y_dev)

    def shared(ref, sem):
        return pltpu.make_async_remote_copy(
            src_ref=ref, dst_ref=ref, send_sem=sem.at[0], recv_sem=b_sem.at[1],
            device_id=y_dev, device_id_type=MESH,
        )

    tok_all.wait_send()
    others = pl.ds(0, (tp - 1) * tok_rows)
    pl.when(at_end)(shared(parts.at[pl.ds(0, tiles - 2 * n), others], ps_sem).wait_send)
    pl.when(jnp.logical_not(at_end))(shared(parts.at[:, others], ps_sem).wait_send)
    pl.when(by_end)(shared(parts_far.at[:, others], p_sem).wait_send)
    pl.when(at_end)(hid_copy.wait_send)
    pl.when(by_end)(sum_copy.wait_send)


def emit_kernel(
    fg, fu, fd, mixed, pg_ref, pb_ref, go_ref, uo_ref, do_ref, res_ref, res, sem, res_sem
):
    tiles = fg.shape[0]
    copies = [
        pltpu.make_async_copy(src.at[k], out.at[:, k * LANES:(k + 1) * LANES], sem.at[m, k])
        for m, (src, out) in enumerate(((fg, go_ref), (fu, uo_ref), (fd, do_ref)))
        for k in range(tiles)
    ]
    for copy in copies:
        copy.start()
    mix = mixed[...]
    center = jnp.mean(mix, axis=-1, keepdims=True)
    off = mix - center
    spread = jnp.mean(jnp.square(off), axis=-1, keepdims=True)
    res[...] = (
        off * lax.rsqrt(spread + 1e-05) * pg_ref[...] + pb_ref[...]
    ).astype(jnp.bfloat16)
    put = pltpu.make_async_copy(res, res_ref, res_sem)
    put.start()
    for copy in copies:
        copy.wait()
    put.wait()


def fused(fs, tp, n, tokens, gate_master, up_master, down_master, norm_gain, post_gain, post_bias):
    rc, cols = gate_master.shape
    tok_rows, d = tokens.shape
    tiles, rows = d // LANES, tp * tok_rows
    bf, f32 = jnp.bfloat16, jnp.float32
    held = pltpu.VMEM((tiles, cols, LANES), bf)
    vmem = pl.BlockSpec(memory_space=pltpu.VMEM)
    anywhere = pl.BlockSpec(memory_space=pl.ANY)
    dma = pltpu.SemaphoreType.DMA
    sources = (tokens, gate_master.T, up_master.T, down_master.T, norm_gain[None, :])
    kept = pl.pallas_call(
        functools.partial(gather_kernel, fs, tp, n),
        out_shape=(held, held, held, pltpu.VMEM((tok_rows, d), f32)),
        in_specs=[anywhere] * 5,
        out_specs=(vmem,) * 4,
        scratch_shapes=[
            pltpu.VMEM((3, 2 * n, cols, LANES), f32),
            pltpu.VMEM((tok_rows, d), bf),
            pltpu.VMEM((1, d), f32),
            pltpu.VMEM((tp, tok_rows, d), bf),
            pltpu.VMEM((rows, cols), f32),
            pltpu.VMEM((rows, cols), f32),
            pltpu.VMEM((rows, cols), bf),
            pltpu.VMEM((tiles, rows, LANES), bf),
            pltpu.VMEM((tp, tiles, tok_rows, LANES), bf),
            pltpu.VMEM((rows, cols), bf),
            pltpu.VMEM((2 * n, rows, LANES), bf),
            pltpu.VMEM((tp - 1, 2 * n, tok_rows, LANES), bf),
            pltpu.VMEM((2 * n, tok_rows, LANES), bf),
            pltpu.VMEM((2 * n, tok_rows, LANES), bf),
            dma((5,)), dma((5,)), dma((5,)), dma((3 * (fs - 1) * n, 2)), dma((fs - 1, 5)),
            dma((2,)), dma((1,)), dma((fs,)), dma((2 * n + 2,)), dma((2,)),
            dma((2,)), dma((2,)), dma((2,)),
        ],
        compiler_params=pltpu.CompilerParams(
            collective_id=0, has_side_effects=True, vmem_limit_bytes=50 * 2**20
        ),
    )(*(pltpu.with_memory_space_constraint(x, pltpu.HBM) for x in sources))
    ready = jax.ShapeDtypeStruct((cols, d), bf)
    gate, up, down, result = pl.pallas_call(
        emit_kernel,
        out_shape=(ready, ready, ready, jax.ShapeDtypeStruct((tok_rows, d), bf)),
        in_specs=[vmem] * 6,
        out_specs=(anywhere,) * 4,
        scratch_shapes=[
            pltpu.VMEM((tok_rows, d), bf), dma((3, tiles)), pltpu.SemaphoreType.DMA,
        ],
        compiler_params=pltpu.CompilerParams(vmem_limit_bytes=20 * 2**20),
    )(
        *(pltpu.with_memory_space_constraint(x, pltpu.VMEM) for x in kept),
        post_gain[None, :], post_bias[None, :],
    )
    return gate.T, up.T, down.T, result


def solution(mesh):
    grp, fs, tp = mesh.shape["grp"], mesh.shape["fs"], mesh.shape["tp"]

    def local(tokens, gate_master, *rest):
        rc, cols = gate_master.shape
        n = rc // (2 * LANES)
        fits = grp == 2 and fs > 3 and rc % (2 * LANES) == 0 and 2 * n * fs <= 32
        fits = fits and cols % 16 == 0 and tokens.shape[0] % 16 == 0
        fits = fits and cols >= 2 * LANES
        if fits:
            return fused(fs, tp, n, tokens, gate_master, *rest)
        return plain(tokens, gate_master, *rest)

    return jax.shard_map(
        local,
        mesh=mesh,
        in_specs=(
            P(("grp", "fs", "tp"), None),
            P("fs", "tp"),
            P("fs", "tp"),
            P("fs", "tp"),
            P(),
            P(),
            P(),
        ),
        out_specs=(P("grp", "tp"), P("grp", "tp"), P("grp", "tp"), P(("grp", "fs", "tp"), None)),
        check_vma=False,
    )
```

time: 85.9 us -> 82.3 us (0.958)
  Pallas kernels: 85 us -> 81.5 us
    pallas_call x1, Pallas kernels: 81.2 us -> 77.7 us  [fused(): pl.pallas_call(functools.partial(gather_kernel, fs, tp, n), out_shape=(he...]
where the time goes in v3:
time: 82.3 us; the launch traced here: 82.2 us
  Pallas kernels  81.5 us (99%)
    pallas_call x1, Pallas kernels, fused(): pl.pallas_call(functools.partial(gather_kernel, fs, tp, n), out_shape=(he...  77.7 us
    pallas_call x1, Pallas kernels, fused(): pl.pallas_call(emit_kernel, out_shape=(ready, ready, ready, jax.ShapeDtyp...  3.81 us

profile of v3, /device:TPU:0, one launch (start us, length us, event | category | flops | bytes accessed | tf_op | source)
XLA Modules:
  0.0 82.2 jit_solution(11070794789816194625)
XLA Ops:
  0.6 0.0 copy-start.1
  0.6 0.0 copy-start
  0.7 77.7 %shard_map.102 = (bf16[16,688,128]{2,1,0:T(8,128)(2,1)S(1)}, bf16[16,688,128]{2,1,0:T(8,128)(2,1)S(1)}, bf16[16,688,128]{2,1,0:T(8,128)(2,1)S(1)}, f32[64,2048]{1,0:T(8,128)S(1)}) custom-call(bf16[64,2048]{1,0:T(8,128)(2,1)} %tok_ref.1, f32[688,512]{1,0:T(8,128)} %bitcast.11, f32[688,512]{1,0:T(8,128)} %bitcast.12, f32[688,512]{1,0:T(8,128)} %bitcast.13, ...), custom_call_target="tpu_custom_call" | custom-call | tf_op jit(solution)/shard_map/pallas_call | solution.py:547
  78.3 0.0 copy-done.1
  78.4 0.0 copy-done
  78.4 3.8 %shard_map.103 = (bf16[688,2048]{1,0:T(8,128)(2,1)}, bf16[688,2048]{1,0:T(8,128)(2,1)}, bf16[688,2048]{1,0:T(8,128)(2,1)}, bf16[64,2048]{1,0:T(8,128)(2,1)}) custom-call(bf16[16,688,128]{2,1,0:T(8,128)(2,1)S(1)} %get-tuple-element.12.fg, bf16[16,688,128]{2,1,0:T(8,128)(2,1)S(1)} %get-tuple-element.13.fu, bf16[16,688,128]{2,1,0:T(8,128)(2,1)S(1)} %get-tuple-element.14.fd, ...), custom_call_target="tpu_custom_call" | custom-call | tf_op jit(solution)/shard_map/pallas_call | solution.py:576
Async XLA Ops:
  0.6 77.7 %copy-start.1 = (f32[2048]{0:T(1024)S(1)}, f32[2048]{0:T(1024)}, u32[]{:S(2)}) copy-start(f32[2048]{0:T(1024)} %param.13) | copy-start | bytes 24580
  0.6 77.7 %copy-start = (f32[2048]{0:T(1024)S(1)}, f32[2048]{0:T(1024)}, u32[]{:S(2)}) copy-start(f32[2048]{0:T(1024)} %param.12) | copy-start | bytes 24580

commit v4 on v3

--- a/solution.py
+++ b/solution.py
@@ -418,6 +418,7 @@
                 arrived(m, c, q, p)
                 if is_last(m, c, q):
                     doubled(c, q, p)
+                work(downs, 2)
             if p == 0 and c == 0:
                 settle(0)
                 work(sums, len(sums))
@@ -429,7 +430,6 @@
             later(m, c, p, y)
             waiting.append((m, c, p))
             settle(1)
-            work(downs, 4)
 
     def far_tile(h, c):
         return tile_of(far, h, c)
@@ -442,13 +442,12 @@
         if not is_last(2, c, q):
             hop(2, c, k, q, y_dev, y_sem, far_skip, True).start()
 
-    @pl.when(at_end)
-    def _():
-        for _, c, q in late[:-1]:
-            far_take(c, q)
-
+    for _, c, q in late[:-2]:
+        pl.when(at_end)(lambda c=c, q=q: far_take(c, q))
+        work(downs, 2)
     settle(0)
     work(downs, len(downs))
+    pl.when(at_end)(lambda: far_take(*late[-2][1:]))
     pl.when(by_end)(help_down)
     work(fins, len(fins))
     pl.when(by_end)(help_sum)
@@ -513,13 +512,11 @@
     fg, fu, fd, mixed, pg_ref, pb_ref, go_ref, uo_ref, do_ref, res_ref, res, sem, res_sem
 ):
     tiles = fg.shape[0]
-    copies = [
-        pltpu.make_async_copy(src.at[k], out.at[:, k * LANES:(k + 1) * LANES], sem.at[m, k])
-        for m, (src, out) in enumerate(((fg, go_ref), (fu, uo_ref), (fd, do_ref)))
-        for k in range(tiles)
-    ]
-    for copy in copies:
-        copy.start()
+    outs = (go_ref, uo_ref, do_ref)
+    for m, src in enumerate((fg, fu, fd)):
+        for k in range(tiles):
+            at = slice(k * LANES, (k + 1) * LANES)
+            pltpu.make_async_copy(src.at[k], outs[m].at[:, at], sem.at[m]).start()
     mix = mixed[...]
     center = jnp.mean(mix, axis=-1, keepdims=True)
     off = mix - center
@@ -529,8 +526,8 @@
     ).astype(jnp.bfloat16)
     put = pltpu.make_async_copy(res, res_ref, res_sem)
     put.start()
-    for copy in copies:
-        copy.wait()
+    for m, out in enumerate(outs):
+        pltpu.make_async_copy(out, out, sem.at[m]).wait()
     put.wait()
 
 
@@ -579,7 +576,7 @@
         in_specs=[vmem] * 6,
         out_specs=(anywhere,) * 4,
         scratch_shapes=[
-            pltpu.VMEM((tok_rows, d), bf), dma((3, tiles)), pltpu.SemaphoreType.DMA,
+            pltpu.VMEM((tok_rows, d), bf), dma((3,)), pltpu.SemaphoreType.DMA,
         ],
         compiler_params=pltpu.CompilerParams(vmem_limit_bytes=20 * 2**20),
     )(

time: 82.3 us -> 81.9 us (level)
  no operation moved by 1% of the time
where the time goes in v4:
time: 81.9 us; the launch traced here: 81.8 us
  Pallas kernels  81.1 us (99%)
    pallas_call x1, Pallas kernels, fused(): pl.pallas_call(functools.partial(gather_kernel, fs, tp, n), out_shape=(he...  77.7 us
    pallas_call x1, Pallas kernels, fused(): pl.pallas_call(emit_kernel, out_shape=(ready, ready, ready, jax.ShapeDtyp...  3.41 us

profile of v4, /device:TPU:0, one launch (start us, length us, event | category | flops | bytes accessed | tf_op | source)
XLA Modules:
  0.0 81.8 jit_solution(9966639624990952739)
XLA Ops:
  0.6 0.0 copy-start.1
  0.6 0.0 copy-start
  0.7 77.7 %shard_map.102 = (bf16[16,688,128]{2,1,0:T(8,128)(2,1)S(1)}, bf16[16,688,128]{2,1,0:T(8,128)(2,1)S(1)}, bf16[16,688,128]{2,1,0:T(8,128)(2,1)S(1)}, f32[64,2048]{1,0:T(8,128)S(1)}) custom-call(bf16[64,2048]{1,0:T(8,128)(2,1)} %tok_ref.1, f32[688,512]{1,0:T(8,128)} %bitcast.11, f32[688,512]{1,0:T(8,128)} %bitcast.12, f32[688,512]{1,0:T(8,128)} %bitcast.13, ...), custom_call_target="tpu_custom_call" | custom-call | tf_op jit(solution)/shard_map/pallas_call | solution.py:544
  78.4 0.0 copy-done.1
  78.4 0.0 copy-done
  78.4 3.4 %shard_map.103 = (bf16[688,2048]{1,0:T(8,128)(2,1)}, bf16[688,2048]{1,0:T(8,128)(2,1)}, bf16[688,2048]{1,0:T(8,128)(2,1)}, bf16[64,2048]{1,0:T(8,128)(2,1)}) custom-call(bf16[16,688,128]{2,1,0:T(8,128)(2,1)S(1)} %get-tuple-element.12.fg, bf16[16,688,128]{2,1,0:T(8,128)(2,1)S(1)} %get-tuple-element.13.fu, bf16[16,688,128]{2,1,0:T(8,128)(2,1)S(1)} %get-tuple-element.14.fd, ...), custom_call_target="tpu_custom_call" | custom-call | tf_op jit(solution)/shard_map/pallas_call | solution.py:573
Async XLA Ops:
  0.6 77.7 %copy-start.1 = (f32[2048]{0:T(1024)S(1)}, f32[2048]{0:T(1024)}, u32[]{:S(2)}) copy-start(f32[2048]{0:T(1024)} %param.13) | copy-start | bytes 24580
  0.6 77.7 %copy-start = (f32[2048]{0:T(1024)S(1)}, f32[2048]{0:T(1024)}, u32[]{:S(2)}) copy-start(f32[2048]{0:T(1024)} %param.12) | copy-start | bytes 24580

commit v5 on v4

--- a/solution.py
+++ b/solution.py
@@ -168,28 +168,28 @@
     def send_dn(m, h, c, q):
         hop(m, c, tile_of(z, h, c), q, dn_dev, dn_sem, 1, h is not y).start()
 
-    def part_copy(b, h, j, peer):
+    def part_copy(b, h, count, j, peer):
         k = tile_of(b, h, 0)
         return pltpu.make_async_remote_copy(
             src_ref=parts.at[
-                pl.ds(k, n), pl.ds(pl.multiple_of(peer * tok_rows, tok_rows), tok_rows)
+                pl.ds(k, count), pl.ds(pl.multiple_of(peer * tok_rows, tok_rows), tok_rows)
             ],
-            dst_ref=got.at[t, pl.ds(k, n)],
+            dst_ref=got.at[t, pl.ds(k, count)],
             send_sem=ps_sem.at[0], recv_sem=pr_sem.at[b],
             device_id=(y, z, peer), device_id_type=MESH,
         )
 
-    def product(lhs, k, to, at):
-        rhs = jnp.concatenate([fd[k + i] for i in range(n)], axis=1)
+    def product(lhs, k, count, to, at):
+        rhs = jnp.concatenate([fd[k + i] for i in range(count)], axis=1)
         part = jnp.dot(lhs[...], rhs, preferred_element_type=jnp.float32)
-        for i in range(n):
+        for i in range(count):
             to[at + i] = part[:, i * LANES:(i + 1) * LANES].astype(jnp.bfloat16)
 
-    def down_half(b, h):
+    def down_half(b, h, count=n):
         k = tile_of(b, h, 0)
-        product(hid, k, parts, k)
+        product(hid, k, count, parts, k)
         for j, peer in enumerate(peers):
-            part_copy(b, h, j, peer).start()
+            part_copy(b, h, count, j, peer).start()
 
     def add_tiles(m, k, start):
         acc = (acc_g, acc_u)[m]
@@ -208,14 +208,14 @@
         wide = own[:, at].astype(jnp.float32)
         mixed[:, at] = jnp.sqrt(jnp.float32(2.0)) * wide + 0.5 * branch
 
-    def finish_origin(b):
-        k = tile_of(b, 0, 0)
-        ref = got.at[pl.ds(0, tp - 1), pl.ds(k, 2 * n)]
+    def finish_origin(b, h=0, count=2 * n):
+        k = tile_of(b, h, 0)
+        ref = got.at[pl.ds(0, tp - 1), pl.ds(k, count)]
         pltpu.make_async_remote_copy(
             src_ref=ref, dst_ref=ref, send_sem=ps_sem.at[0], recv_sem=pr_sem.at[b],
             device_id=y_dev, device_id_type=MESH,
         ).wait_recv()
-        for i in range(2 * n):
+        for i in range(count):
             branch = parts[k + i, mine, :].astype(jnp.float32)
             for peer in senders:
                 branch = branch + got[peer, k + i].astype(jnp.float32)
@@ -241,8 +241,8 @@
 
     def help_down():
         hid_copy.wait_recv()
-        for h in (0, 1):
-            product(hid_far, tile_of(far, h, 0), parts_far, h * n)
+        product(hid_far, tile_of(far, cross, 0), n, parts_far, 0)
+        product(hid_far, tile_of(far, y, n - 1), 1, parts_far, n)
         for j, peer in enumerate(peers):
             far_copy(j, peer).start()
 
@@ -445,6 +445,9 @@
     for _, c, q in late[:-2]:
         pl.when(at_end)(lambda c=c, q=q: far_take(c, q))
         work(downs, 2)
+    if n > 1:
+        downs.append((at_end, lambda: down_half(far, y, n - 1)))
+        fins.append((at_end, lambda: finish_origin(far, y, n - 1)))
     settle(0)
     work(downs, len(downs))
     pl.when(at_end)(lambda: far_take(*late[-2][1:]))
@@ -458,8 +461,9 @@
         for g in (2, 3, 4) if n > 1 else (3, 4):
             crossed_all(2, far, g, far_skip)
         sum_copy.wait_recv()
-        for i in range(2 * n):
-            mix(far * (2 * n) + i, branch_far[i].astype(jnp.float32))
+        for i in range(n):
+            mix(far_tile(cross, i), branch_far[i].astype(jnp.float32))
+        mix(far_tile(y, n - 1), branch_far[n].astype(jnp.float32))
 
     def sent(g, count, sem, dev):
         if count:
@@ -501,7 +505,7 @@
 
     tok_all.wait_send()
     others = pl.ds(0, (tp - 1) * tok_rows)
-    pl.when(at_end)(shared(parts.at[pl.ds(0, tiles - 2 * n), others], ps_sem).wait_send)
+    pl.when(at_end)(shared(parts.at[pl.ds(0, tiles - n - 1), others], ps_sem).wait_send)
     pl.when(jnp.logical_not(at_end))(shared(parts.at[:, others], ps_sem).wait_send)
     pl.when(by_end)(shared(parts_far.at[:, others], p_sem).wait_send)
     pl.when(at_end)(hid_copy.wait_send)
@@ -557,10 +561,10 @@
             pltpu.VMEM((tiles, rows, LANES), bf),
             pltpu.VMEM((tp, tiles, tok_rows, LANES), bf),
             pltpu.VMEM((rows, cols), bf),
-            pltpu.VMEM((2 * n, rows, LANES), bf),
-            pltpu.VMEM((tp - 1, 2 * n, tok_rows, LANES), bf),
-            pltpu.VMEM((2 * n, tok_rows, LANES), bf),
-            pltpu.VMEM((2 * n, tok_rows, LANES), bf),
+            pltpu.VMEM((n + 1, rows, LANES), bf),
+            pltpu.VMEM((tp - 1, n + 1, tok_rows, LANES), bf),
+            pltpu.VMEM((n + 1, tok_rows, LANES), bf),
+            pltpu.VMEM((n + 1, tok_rows, LANES), bf),
             dma((5,)), dma((5,)), dma((5,)), dma((3 * (fs - 1) * n, 2)), dma((fs - 1, 5)),
             dma((2,)), dma((1,)), dma((fs,)), dma((2 * n + 2,)), dma((2,)),
             dma((2,)), dma((2,)), dma((2,)),

time: 81.9 us -> 81.6 us (level)
  no operation moved by 1% of the time
where the time goes in v5:
time: 81.6 us; the launch traced here: 81.4 us
  Pallas kernels  80.7 us (99%)
    pallas_call x1, Pallas kernels, fused(): pl.pallas_call(functools.partial(gather_kernel, fs, tp, n), out_shape=(he...  77.3 us
    pallas_call x1, Pallas kernels, fused(): pl.pallas_call(emit_kernel, out_shape=(ready, ready, ready, jax.ShapeDtyp...  3.41 us

profile of v5, /device:TPU:0, one launch (start us, length us, event | category | flops | bytes accessed | tf_op | source)
XLA Modules:
  0.0 81.4 jit_solution(9389291523642289934)
XLA Ops:
  0.6 0.0 copy-start.1
  0.6 0.0 copy-start
  0.7 77.3 %shard_map.102 = (bf16[16,688,128]{2,1,0:T(8,128)(2,1)S(1)}, bf16[16,688,128]{2,1,0:T(8,128)(2,1)S(1)}, bf16[16,688,128]{2,1,0:T(8,128)(2,1)S(1)}, f32[64,2048]{1,0:T(8,128)S(1)}) custom-call(bf16[64,2048]{1,0:T(8,128)(2,1)} %tok_ref.1, f32[688,512]{1,0:T(8,128)} %bitcast.11, f32[688,512]{1,0:T(8,128)} %bitcast.12, f32[688,512]{1,0:T(8,128)} %bitcast.13, ...), custom_call_target="tpu_custom_call" | custom-call | tf_op jit(solution)/shard_map/pallas_call | solution.py:548
  78.0 0.0 copy-done.1
  78.0 0.0 copy-done
  78.0 3.4 %shard_map.103 = (bf16[688,2048]{1,0:T(8,128)(2,1)}, bf16[688,2048]{1,0:T(8,128)(2,1)}, bf16[688,2048]{1,0:T(8,128)(2,1)}, bf16[64,2048]{1,0:T(8,128)(2,1)}) custom-call(bf16[16,688,128]{2,1,0:T(8,128)(2,1)S(1)} %get-tuple-element.12.fg, bf16[16,688,128]{2,1,0:T(8,128)(2,1)S(1)} %get-tuple-element.13.fu, bf16[16,688,128]{2,1,0:T(8,128)(2,1)S(1)} %get-tuple-element.14.fd, ...), custom_call_target="tpu_custom_call" | custom-call | tf_op jit(solution)/shard_map/pallas_call | solution.py:577
Async XLA Ops:
  0.6 77.4 %copy-start.1 = (f32[2048]{0:T(1024)S(1)}, f32[2048]{0:T(1024)}, u32[]{:S(2)}) copy-start(f32[2048]{0:T(1024)} %param.13) | copy-start | bytes 24580
  0.6 77.4 %copy-start = (f32[2048]{0:T(1024)S(1)}, f32[2048]{0:T(1024)}, u32[]{:S(2)}) copy-start(f32[2048]{0:T(1024)} %param.12) | copy-start | bytes 24580

commit v6 on v5

--- a/solution.py
+++ b/solution.py
@@ -58,7 +58,7 @@
     fg, fu, fd, mixed,
     stage, own, gain, toks, acc_g, acc_u, hid, parts, got,
     hid_far, parts_far, got_far, sum_far, branch_far,
-    up_sem, dn_sem, y_sem, r_sem, x_sem, t_sem, ps_sem, pr_sem, i_sem, l_sem, h_sem, p_sem, b_sem,
+    up_sem, dn_sem, y_sem, r_sem, x_sem, t_sem, ps_sem, pr_sem, i_sem, l_sem, p_sem, b_sem,
 ):
     y, z, t = lax.axis_index("grp"), lax.axis_index("fs"), lax.axis_index("tp")
     cols, rc = gm_ref.shape
@@ -98,7 +98,7 @@
         return (m, c, q[0]) == (2, n - 1, 1)
 
     def group(m, c, q):
-        return m if (m, c) != (2, n - 1) else 3 + q[0]
+        return max(m - 1, 0) if (m, c) != (2, n - 1) else 2 + q[0]
 
     def fetch(m, h, c, slot):
         k = h * n + c
@@ -140,12 +140,14 @@
             device_id=dev, device_id_type=MESH,
         )
 
-    def crossed_all(m, b, g, skip):
+    def crossed_all(b, g, skip):
         k = tile_of(b, cross, 0)
-        if g < 3:
-            ref = full[m].at[pl.ds(k, (n, n, n - 1)[g])]
+        if g == 0:
+            ref = full[0].at[pl.ds(tile_of(b, 0, 0), 2 * n)]
+        elif g == 1:
+            ref = full[2].at[pl.ds(k, n - 1)]
         else:
-            q = pieces[g - 3]
+            q = pieces[g - 2]
             ref = full[2].at[k + n - 1, pl.ds(q[1], q[2])]
         pltpu.make_async_remote_copy(
             src_ref=ref, dst_ref=ref, send_sem=y_sem.at[g], recv_sem=x_sem.at[b - skip, g],
@@ -222,7 +224,7 @@
             mix(k + i, branch)
 
     hid_copy = pltpu.make_async_remote_copy(
-        src_ref=hid, dst_ref=hid_far, send_sem=h_sem.at[0], recv_sem=h_sem.at[1],
+        src_ref=hid, dst_ref=hid_far, send_sem=b_sem.at[0], recv_sem=b_sem.at[1],
         device_id=helper, device_id_type=MESH,
     )
     sum_copy = pltpu.make_async_remote_copy(
@@ -297,7 +299,7 @@
 
     def doubled(c, q, p):
         def take_other(b, more, dev, sem, skip):
-            crossed_all(2, b, 4, skip)
+            crossed_all(b, 3, skip)
             k = tile_of(b, cross, c)
             pl.when(more)(lambda: hop(2, c, k, q, dev, sem, skip, True).start())
 
@@ -310,11 +312,11 @@
         )
 
     def crossed(m, c, p):
-        groups = {n - 1: (m,) if m < 2 else (3, 4), n - 2: () if m < 2 else (2,)}.get(c, ())
+        groups = {(1, n - 1): (0,), (2, n - 1): (2, 3), (2, n - 2): (1,)}.get((m, c), ())
         for skip, (b, ok, b_end) in enumerate(ends(p)):
             for g in groups:
-                here = jnp.logical_and(ok, jnp.logical_not(b_end)) if g == 4 else ok
-                pl.when(here)(lambda b=b, g=g, skip=skip: crossed_all(m, b, g, skip))
+                here = jnp.logical_and(ok, jnp.logical_not(b_end)) if g == 3 else ok
+                pl.when(here)(lambda b=b, g=g, skip=skip: crossed_all(b, g, skip))
 
     def later(m, c, p, h):
         if c < n - 1:
@@ -325,7 +327,8 @@
                 if h is not y:
                     fins.append((ok, lambda b=b: finish_origin(b)))
             else:
-                sums.append((ok, lambda b=b: add_tiles(m, tile_of(b, h, 0), False)))
+                for w in (m,) if h is y else (0, 1) if m == 1 else ():
+                    sums.append((ok, lambda b=b, w=w: add_tiles(w, tile_of(b, h, 0), False)))
 
     def tok_copy(peer, origin):
         return pltpu.make_async_remote_copy(
@@ -458,8 +461,8 @@
     @pl.when(at_end)
     def _():
         far_take(*late[-1][1:])
-        for g in (2, 3, 4) if n > 1 else (3, 4):
-            crossed_all(2, far, g, far_skip)
+        for g in (1, 2, 3) if n > 1 else (2, 3):
+            crossed_all(far, g, far_skip)
         sum_copy.wait_recv()
         for i in range(n):
             mix(far_tile(cross, i), branch_far[i].astype(jnp.float32))
@@ -467,31 +470,31 @@
 
     def sent(g, count, sem, dev):
         if count:
-            rows = (slice(0, cols),) * 3 + (slice(0, middle), slice(middle, cols))
+            rows = (slice(0, cols),) * 2 + (slice(0, middle), slice(middle, cols))
             rows = rows[g]
-            ref = full[min(g, 2)].at[pl.ds(0, count), rows]
+            ref = full[2 if g else 0].at[pl.ds(0, count), rows]
             pltpu.make_async_remote_copy(
                 src_ref=ref, dst_ref=ref, send_sem=sem.at[g], recv_sem=b_sem.at[1],
                 device_id=dev, device_id_type=MESH,
             ).wait_send()
 
     def sends(j, g):
-        base = (n, n, n - 1, 1, 1)[g]
+        base = (2 * n, n - 1, 1, 1)[g]
         outer = (0, fs - 1)
-        twice = lambda b: 2 * base if g == 4 and b in outer else base
+        twice = lambda b: 2 * base if g == 3 and b in outer else base
         mine = 2 * base if j in outer else base
         up = mine + sum(twice(b) for b in range(j)) if j < fs - 1 else 0
         dn = mine + sum(twice(b) for b in range(j + 1, fs)) if j > 0 else 0
         cross = sum(
             base for b in range(fs)
-            if b != j and not (b in outer and (abs(b - j) == 1 or g == 4))
+            if b != j and not (b in outer and (abs(b - j) == 1 or g == 3))
         )
         return up, dn, cross
 
     for j in range(fs):
         @pl.when(z == j)
         def _(j=j):
-            for g in range(5):
+            for g in range(4):
                 up, dn, cross = sends(j, g)
                 sent(g, up, up_sem, up_dev)
                 sent(g, dn, dn_sem, dn_dev)
@@ -565,9 +568,9 @@
             pltpu.VMEM((tp - 1, n + 1, tok_rows, LANES), bf),
             pltpu.VMEM((n + 1, tok_rows, LANES), bf),
             pltpu.VMEM((n + 1, tok_rows, LANES), bf),
-            dma((5,)), dma((5,)), dma((5,)), dma((3 * (fs - 1) * n, 2)), dma((fs - 1, 5)),
+            dma((4,)), dma((4,)), dma((4,)), dma((3 * (fs - 1) * n, 2)), dma((fs - 1, 4)),
             dma((2,)), dma((1,)), dma((fs,)), dma((2 * n + 2,)), dma((2,)),
-            dma((2,)), dma((2,)), dma((2,)),
+            dma((2,)), dma((2,)),
         ],
         compiler_params=pltpu.CompilerParams(
             collective_id=0, has_side_effects=True, vmem_limit_bytes=50 * 2**20

time: 81.6 us -> 81.5 us (level)
  no operation moved by 1% of the time
where the time goes in v6:
time: 81.5 us; the launch traced here: 81.3 us
  Pallas kernels  80.7 us (99%)
    pallas_call x1, Pallas kernels, fused(): pl.pallas_call(functools.partial(gather_kernel, fs, tp, n), out_shape=(he...  77.2 us
    pallas_call x1, Pallas kernels, fused(): pl.pallas_call(emit_kernel, out_shape=(ready, ready, ready, jax.ShapeDtyp...  3.41 us

profile of v6, /device:TPU:0, one launch (start us, length us, event | category | flops | bytes accessed | tf_op | source)
XLA Modules:
  0.0 81.3 jit_solution(6955634196053563033)
XLA Ops:
  0.6 0.0 copy-start.1
  0.6 0.0 copy-start
  0.7 77.2 %shard_map.102 = (bf16[16,688,128]{2,1,0:T(8,128)(2,1)S(1)}, bf16[16,688,128]{2,1,0:T(8,128)(2,1)S(1)}, bf16[16,688,128]{2,1,0:T(8,128)(2,1)S(1)}, f32[64,2048]{1,0:T(8,128)S(1)}) custom-call(bf16[64,2048]{1,0:T(8,128)(2,1)} %tok_ref.1, f32[688,512]{1,0:T(8,128)} %bitcast.11, f32[688,512]{1,0:T(8,128)} %bitcast.12, f32[688,512]{1,0:T(8,128)} %bitcast.13, ...), custom_call_target="tpu_custom_call" | custom-call | tf_op jit(solution)/shard_map/pallas_call | solution.py:551
  77.9 0.0 copy-done.1
  77.9 0.0 copy-done
  77.9 3.4 %shard_map.103 = (bf16[688,2048]{1,0:T(8,128)(2,1)}, bf16[688,2048]{1,0:T(8,128)(2,1)}, bf16[688,2048]{1,0:T(8,128)(2,1)}, bf16[64,2048]{1,0:T(8,128)(2,1)}) custom-call(bf16[16,688,128]{2,1,0:T(8,128)(2,1)S(1)} %get-tuple-element.12.fg, bf16[16,688,128]{2,1,0:T(8,128)(2,1)S(1)} %get-tuple-element.13.fu, bf16[16,688,128]{2,1,0:T(8,128)(2,1)S(1)} %get-tuple-element.14.fd, ...), custom_call_target="tpu_custom_call" | custom-call | tf_op jit(solution)/shard_map/pallas_call | solution.py:580
Async XLA Ops:
  0.6 77.3 %copy-start.1 = (f32[2048]{0:T(1024)S(1)}, f32[2048]{0:T(1024)}, u32[]{:S(2)}) copy-start(f32[2048]{0:T(1024)} %param.13) | copy-start | bytes 24580
  0.6 77.3 %copy-start = (f32[2048]{0:T(1024)S(1)}, f32[2048]{0:T(1024)}, u32[]{:S(2)}) copy-start(f32[2048]{0:T(1024)} %param.12) | copy-start | bytes 24580
